TPU v7x, 128 devices: a whole 4x4x4 slice. The times are simulated.
128 devices in a mesh: sp: 32 (over z, y, core), tp: 4 (over x).
Axes of the slice: x: 4, y: 4, z: 4, core: 2. Of those that a mesh axis runs over, the one named last changes fastest.
Arguments:
- residual: bfloat16 [12288, 2048], P('sp'), may hold values from -50 to 50
- queries_a: bfloat16 [12288, 512], P('sp', 'tp'), may hold values from -50 to 50
- keys_a: bfloat16 [12288, 512], P('sp', 'tp'), may hold values from -9 to 9
- values_a: bfloat16 [12288, 512], P('sp', 'tp'), may hold values from -6 to 6
- queries_b: bfloat16 [12288, 1024], P('sp', 'tp'), may hold values from -50 to 50
- keys_b: bfloat16 [12288, 1024], P('sp', 'tp'), may hold values from -9 to 9
- values_b: bfloat16 [12288, 512], P('sp', 'tp'), may hold values from -6 to 6
- mix_lambda: float32 [2, 4], P(None, 'tp'), may hold values from 0.3 to 0.8
- head_gain: float32 [2, 128], replicated, may hold values from 0.1 to 1.9
- out_a: bfloat16 [512, 2048], P('tp'), may hold values from -0.1875 to 0.1875
- out_b: bfloat16 [512, 2048], P('tp'), may hold values from -0.1875 to 0.1875
- norm_gain: float32 [2048], replicated, may hold values from 0.1 to 1.9
- w_gate: bfloat16 [2048, 5632], P('sp', 'tp'), may hold values from -0.125 to 0.125
- w_up: bfloat16 [2048, 5632], P('sp', 'tp'), may hold values from -0.125 to 0.125
- w_down: bfloat16 [5632, 2048], P('tp', 'sp'), may hold values from -0.21875 to 0.21875
Outputs:
- layer_out: bfloat16 [12288, 2048], P('sp', 'tp')
All inputs are finite; a program needn't handle non-finite values.
Results may differ from a plain program's by a relative error of at most 0.0085.
Values may be sent and summed in bfloat16 or wider, within the bound.
No kernel may reach another device: no remote copies, remote signals or barrier semaphores. Data moves between devices by JAX's collectives and lax.ppermute only.
A program may use at most 256 MiB of HBM per device.

v0:
```python
import math
import functools
import jax
import jax.numpy as jnp
from jax import lax
from jax.experimental import pallas as pl
from jax.experimental.pallas import tpu as pltpu
from jax.sharding import PartitionSpec as P

eps_norm = 1e-06
head_scale = 0.8
log2e = math.log2(math.e)
f32 = jnp.float32
bf16 = jnp.bfloat16

SP = [(z, y, c) for z in range(4) for y in range(4) for c in range(2)]


def place(z, y, c):
    return (z % 4) * 8 + (y % 4) * 2 + c % 2


def along_y(x, k):
    return lax.ppermute(x, "sp", [(place(z, y, c), place(z, y + k, c)) for z, y, c in SP])


def along_z(x, k):
    return lax.ppermute(x, "sp", [(place(z, y, c), place(z + k, y, c)) for z, y, c in SP])


def other_core(x):
    return lax.ppermute(x, "sp", [(place(z, y, c), place(z, y, c + 1)) for z, y, c in SP])


def along_x(x, k):
    return lax.ppermute(x, "tp", [(i, (i + k) % 4) for i in range(4)])


def dot(a, b, ca, cb):
    return lax.dot_general(a, b, (((ca,), (cb,)), ((), ())), preferred_element_type=f32)


def pack_body(layout, *refs):
    n = sum(len(parts) for parts in layout)
    ins, outs, sem = refs[:n], refs[n:-1], refs[-1]
    copies, i = [], 0
    for out, parts in zip(outs, layout):
        for corner in parts:
            part = tuple(pl.ds(c, d) for c, d in zip(corner, ins[i].shape))
            copies.append(pltpu.make_async_copy(ins[i], out.at[part], sem.at[i]))
            i += 1
    for c in copies:
        c.start()
    for c in copies:
        c.wait()


def in_hbm(x):
    return pltpu.with_memory_space_constraint(x, pltpu.HBM)


def pack(*sides):
    layout, shapes = [], []
    for arrays, axis in sides:
        at, corners = 0, []
        for a in arrays:
            corners.append((at, 0) if axis == 0 else (0, at))
            at += a.shape[axis]
        other = arrays[0].shape[1 - axis]
        layout.append(corners)
        shapes.append(jax.ShapeDtypeStruct((at, other) if axis == 0 else (other, at), arrays[0].dtype))
    flat = [in_hbm(a) for arrays, _ in sides for a in arrays]
    return pl.pallas_call(
        functools.partial(pack_body, layout),
        out_shape=tuple(shapes),
        in_specs=[pl.BlockSpec(memory_space=pltpu.HBM)] * len(flat),
        out_specs=tuple(pl.BlockSpec(memory_space=pltpu.VMEM) for _ in shapes),
        scratch_shapes=[pltpu.SemaphoreType.DMA((len(flat),))],
        compiler_params=pltpu.CompilerParams(vmem_limit_bytes=8 * MIB),
        name="pack",
    )(*flat)


PER = 2
AHEAD = 3
MIB = 1024 * 1024


def attend_body(groups, m, nk, carry, pick, consts, rows, wa, wb, vd, *refs):
    nq = groups * m
    q_refs, refs = refs[:nq], refs[nq:]
    kv_refs, refs = refs[:nk], refs[nk:]
    if carry:
        acc_in, ml_in, refs = refs[0], refs[1], refs[2:]
    send = pick is not None and pick[2]
    outs = m if send else 2
    q_buf, kv_buf, pad_buf, q_sem, kv_sem, acc_sem = refs[outs : outs + 6]
    turned = None
    rest = refs[outs + 6 :]
    if groups > 1:
        turned, rest = rest[0], rest[1:]
    if send:
        o_refs = refs[:m]
        acc_ref, ml_ref = rest
    else:
        acc_ref, ml_ref = refs[:2]
    q_copies = [
        pltpu.make_async_copy(q_refs[i], q_buf.at[i // m, pl.ds((i % m) * rows, rows)], q_sem.at[i]) for i in range(nq)
    ]
    kv_copies = [
        pltpu.make_async_copy(kv_refs[i], kv_buf.at[pl.ds(i * rows, rows)], kv_sem.at[i]) for i in range(nk)
    ]
    if carry:
        if pick is not None:
            lanes = pl.ds(pick[1] * rows, m * rows)
            acc_in = acc_in.at[pl.ds(pick[0], 1), :, lanes]
            ml_in = ml_in.at[pl.ds(pick[0], 1), :, lanes]
        acc_copies = [
            pltpu.make_async_copy(acc_in, acc_ref, acc_sem.at[0]),
            pltpu.make_async_copy(ml_in, ml_ref, acc_sem.at[1]),
        ]
    else:
        acc_copies = []
    per = min(PER, nk)
    for c in q_copies + kv_copies[:per] + acc_copies + kv_copies[per:]:
        c.start()
    if not carry:
        acc_ref[...] = jnp.zeros_like(acc_ref)
        ml_ref[:, 0:8, :] = jnp.full((groups, 8, m * rows), -jnp.inf, f32)
        ml_ref[:, 8:16, :] = jnp.zeros((groups, 8, m * rows), f32)
    for c in q_copies:
        c.wait()
    for g in range(groups):
        qa = q_buf[g, :, 0 : 2 * wa]
        col = lax.broadcasted_iota(jnp.int32, qa.shape, 1)
        zero = jnp.zeros_like(qa)
        pad_buf[g, :, 0 : 2 * wa] = jnp.where(col < wa, qa, zero)
        pad_buf[g, :, 2 * wa :] = jnp.where(col >= wa, qa, zero)
    for c in acc_copies:
        c.wait()
    steps = nk // per
    tall = per * rows
    wide = m * rows
    lane = 256 if wide % 256 == 0 else wide
    items = [(h, j) for h in range(wide // lane) for j in range(4)]

    def step(t, _):
        qi = t // steps
        ci = t % steps
        keys = pl.ds(pl.multiple_of(ci * tall, tall), tall)

        @pl.when(qi == 0)
        def _():
            for b in range(per):
                i = ci * per + b
                pltpu.make_async_copy(kv_refs[0], kv_buf.at[pl.ds(i * rows, rows)], kv_sem.at[i]).wait()
            if turned is not None:
                first = lax.broadcasted_iota(jnp.int32, (16, tall), 0) == 0
                for g in range(2):
                    at = 2 * wa + 2 * wb + g * vd
                    turned[ci, g, 0:vd, :] = kv_buf[keys, at : at + vd].T
                    turned[ci, g, vd : vd + 16, :] = jnp.where(first, 1.0, 0.0).astype(bf16)

        def score(h, j):
            lanes = slice(h * lane, (h + 1) * lane)
            if j < 2:
                return dot(kv_buf[keys, 0 : 2 * wa], pad_buf[qi, lanes, j * 2 * wa : (j + 1) * 2 * wa], 1, 1)
            at = 2 * wa + (j - 2) * wb
            return dot(kv_buf[keys, at : at + wb], q_buf[qi, lanes, at : at + wb], 1, 1)

        ready = [score(*item) for item in items[:AHEAD]]
        for n, (h, j) in enumerate(items):
            if n + AHEAD < len(items):
                ready.append(score(*items[n + AHEAD]))
            s = ready.pop(0)
            lanes = slice(h * lane, (h + 1) * lane)
            c = consts[j // 2]
            old = ml_ref[qi, j : j + 1, lanes]
            top = jnp.maximum(old, jnp.max(s, axis=0, keepdims=True))
            w = jnp.exp2((s - top) * c)
            decay = jnp.exp2((old - top) * c)
            ml_ref[qi, j : j + 1, lanes] = top
            if turned is not None:
                more = dot(turned[ci, j // 2], w.astype(bf16), 1, 0)
                total = more[vd : vd + 1]
                more = more[0:vd]
            else:
                total = jnp.sum(w, axis=0, keepdims=True)
                at = 2 * wa + 2 * wb + (j // 2) * vd
                more = dot(kv_buf[keys, at : at + vd], w.astype(bf16), 0, 0)
            ml_ref[qi, j + 8 : j + 9, lanes] = ml_ref[qi, j + 8 : j + 9, lanes] * decay + total
            part = slice(j * vd, (j + 1) * vd)
            acc_ref[qi, part, lanes] = acc_ref[qi, part, lanes] * decay + more
        return 0

    lax.fori_loop(0, groups * steps, step, 0)
    if send:
        level = level_of(ml_ref, consts)
        high = level.astype(bf16).astype(f32)
        mid = (level - high).astype(bf16).astype(f32)
        low = level - high - mid
        stats = jnp.concatenate([high, mid, low, jnp.zeros_like(low)], axis=0).astype(bf16)
        for i, o_ref in enumerate(o_refs):
            lanes = slice(i * rows, (i + 1) * rows)
            for j in range(4):
                part = slice(j * vd, (j + 1) * vd)
                inverse = 1.0 / ml_ref[0, j + 8 : j + 9, lanes]
                o_ref[part, :] = (acc_ref[0, part, lanes] * inverse).astype(bf16)
            o_ref[4 * vd :, :] = stats[:, lanes]


def level_of(ml_ref, consts):
    row = lax.broadcasted_iota(jnp.int32, (8, ml_ref.shape[2]), 0)
    used = row < 4
    top = jnp.where(used, ml_ref[0, 0:8, :], 0.0)
    total = jnp.where(used, ml_ref[0, 8:16, :], 1.0)
    return top * jnp.where(row < 2, consts[0], consts[1]) + jnp.log2(total)


def attend(queries, blocks, state, pick, consts, wa, wb, vd):
    groups, m = len(queries), len(queries[0])
    flat = [q for g in queries for q in g]
    nq, nk = len(flat), len(blocks)
    rows = flat[0].shape[0]
    wide = flat[0].shape[1]
    cols = blocks[0].shape[1]
    anywhere = pl.BlockSpec(memory_space=pl.ANY)
    vmem = pl.BlockSpec(memory_space=pltpu.VMEM)
    acc_shape = (groups, 4 * vd, m * rows)
    ml_shape = (groups, 16, m * rows)
    scratch = [
        pltpu.VMEM((groups, m * rows, wide), bf16),
        pltpu.VMEM((nk * rows, cols), bf16),
        pltpu.VMEM((groups, m * rows, 4 * wa), bf16),
        pltpu.SemaphoreType.DMA((nq,)),
        pltpu.SemaphoreType.DMA((nk,)),
        pltpu.SemaphoreType.DMA((2,)),
    ]
    if groups > 1:
        per = min(PER, nk)
        scratch.append(pltpu.VMEM((nk // per, 2, vd + 16, per * rows), bf16))
    if pick is not None and pick[2]:
        out_shape = (jax.ShapeDtypeStruct((4 * vd + 32, rows), bf16),) * m
        out_specs = (vmem,) * m
        scratch += [pltpu.VMEM(acc_shape, f32), pltpu.VMEM(ml_shape, f32)]
    else:
        out_shape = (jax.ShapeDtypeStruct(acc_shape, f32), jax.ShapeDtypeStruct(ml_shape, f32))
        out_specs = (vmem, vmem)
    work = nq * nk * rows * rows
    return pl.pallas_call(
        functools.partial(attend_body, groups, m, nk, state is not None, pick, consts, rows, wa, wb, vd),
        out_shape=out_shape,
        in_specs=[anywhere] * (nq + nk + (0 if state is None else 2)),
        out_specs=out_specs,
        scratch_shapes=scratch,
        compiler_params=pltpu.CompilerParams(vmem_limit_bytes=16 * MIB),
        cost_estimate=pl.CostEstimate(flops=work * 4 * 4 * vd, transcendentals=4 * work, bytes_accessed=nk * rows * cols * 2),
        name="attend",
    )(*flat, *blocks, *(state or ()))


def merge_body(consts, vd, lam_ref, gain_ref, acc_ref, ml_ref, *refs):
    others, out_ref = refs[:-1], refs[-1]
    levels = [level_of(ml_ref, consts)]
    for o in others:
        stats = o[4 * vd :, :].astype(f32)
        levels.append(stats[0:8] + stats[8:16] + stats[16:24])
    top = functools.reduce(jnp.maximum, levels)
    shares = [jnp.exp2(v - top) for v in levels]
    inverse = 1.0 / functools.reduce(jnp.add, shares)
    shares = [v * inverse for v in shares]
    for g in range(2):
        ratio = []
        for j in (2 * g, 2 * g + 1):
            part = slice(j * vd, (j + 1) * vd)
            value = acc_ref[0, part, :] * (shares[0][j : j + 1] / ml_ref[0, j + 8 : j + 9, :])
            for o, share in zip(others, shares[1:]):
                value = value + o[part, :].astype(f32) * share[j : j + 1]
            ratio.append(value)
        mixed = ratio[0] - lam_ref[0:1, g : g + 1] * ratio[1]
        scale = lax.rsqrt(jnp.mean(mixed * mixed, axis=0, keepdims=True) + eps_norm)
        normed = (mixed * scale).T * gain_ref[g : g + 1, :] * head_scale
        out_ref[:, g * vd : (g + 1) * vd] = normed.astype(bf16)


def merge(state, others, lam, gain, consts, vd):
    rows = state[1].shape[-1]
    vmem = pl.BlockSpec(memory_space=pltpu.VMEM)
    return pl.pallas_call(
        functools.partial(merge_body, consts, vd),
        out_shape=jax.ShapeDtypeStruct((rows, 2 * vd), bf16),
        in_specs=[vmem] * (4 + len(others)),
        out_specs=vmem,
        compiler_params=pltpu.CompilerParams(vmem_limit_bytes=12 * MIB),
        name="merge",
    )(lam.T, gain, *state, *others)


def project_body(n, share, *refs):
    at_ref, heads, outs = refs[0], refs[1 : 1 + n], refs[1 + n : 1 + 2 * n]
    residual_ref, gain_ref, normed_ref, cols_ref, summed_ref = refs[1 + 2 * n :]
    total = residual_ref[...].astype(f32)
    for h, o in zip(heads, outs):
        total = total + dot(h[...], o[...], 1, 0)
    summed_ref[...] = total
    inverse = lax.rsqrt(jnp.mean(total * total, axis=-1, keepdims=True) + eps_norm)
    normed_ref[...] = (summed_ref[...] * inverse * gain_ref[...]).astype(bf16)
    cols_ref[...] = summed_ref[:, pl.ds(pl.multiple_of(at_ref[0] * share, share), share)]


def project(at, heads, outs, residual, gain, share):
    n = len(heads)
    rows, wide = residual.shape
    vmem = pl.BlockSpec(memory_space=pltpu.VMEM)
    smem = pl.BlockSpec(memory_space=pltpu.SMEM)
    return pl.pallas_call(
        functools.partial(project_body, n, share),
        out_shape=(jax.ShapeDtypeStruct((rows, wide), bf16), jax.ShapeDtypeStruct((rows, share), f32)),
        in_specs=[smem] + [vmem] * (2 * n + 2),
        out_specs=(vmem, vmem),
        scratch_shapes=[pltpu.VMEM((rows, wide), f32)],
        compiler_params=pltpu.CompilerParams(vmem_limit_bytes=20 * MIB),
        cost_estimate=pl.CostEstimate(flops=2 * rows * wide * n * heads[0].shape[1], transcendentals=0, bytes_accessed=8 * MIB),
        name="project",
    )(at, *heads, *outs, residual, gain)


CUTS = 2


def hidden_body(at_ref, x_ref, w_ref, down_ref, hidden_ref, low_ref, high_ref, sum_ref):
    step = pl.program_id(0)
    spread, _, deep, units = w_ref.shape
    tall = spread * deep
    which, cut = step // CUTS, step % CUTS
    more = dot(x_ref[:, pl.ds(pl.multiple_of(cut * tall, tall), tall)], w_ref[...].reshape(tall, units), 1, 0)

    @pl.when(cut == 0)
    def _():
        sum_ref[which] = more

    @pl.when(cut > 0)
    def _():
        sum_ref[which] = sum_ref[which] + more

    @pl.when(step == 2 * CUTS - 1)
    def _():
        gate = sum_ref[0]
        hidden_ref[...] = (gate / (1.0 + jnp.exp(-gate)) * sum_ref[1]).astype(bf16)
        piece = dot(hidden_ref[...], down_ref[...].reshape(-1, units), 1, 1).astype(bf16)
        half = piece.shape[0] // 2
        low_ref[...] = piece[:half]
        high_ref[...] = piece[half:]


def hidden_of(at, x, w, n):
    rows, wide = x.shape
    spread, _, deep, units = w.shape
    share = wide // n
    whole = lambda p, at: (0, 0)
    return pl.pallas_call(
        hidden_body,
        grid_spec=pltpu.PrefetchScalarGridSpec(
            num_scalar_prefetch=1,
            grid=(2 * CUTS,),
            in_specs=[
                pl.BlockSpec((rows, wide), whole),
                pl.BlockSpec((spread // CUTS, 1, deep, units), lambda p, at: (p % CUTS, p // CUTS, 0, 0)),
                pl.BlockSpec((spread // n, 1, deep, units), lambda p, at: ((at[0] + 2) % n, 2, 0, 0)),
            ],
            out_specs=(
                pl.BlockSpec((rows, units), whole),
                pl.BlockSpec((rows // 2, share), whole),
                pl.BlockSpec((rows // 2, share), whole),
            ),
            scratch_shapes=[pltpu.VMEM((2, rows, units), f32)],
        ),
        out_shape=(
            jax.ShapeDtypeStruct((rows, units), bf16),
            jax.ShapeDtypeStruct((rows // 2, share), bf16),
            jax.ShapeDtypeStruct((rows // 2, share), bf16),
        ),
        compiler_params=pltpu.CompilerParams(vmem_limit_bytes=36 * MIB, dimension_semantics=("arbitrary",)),
        cost_estimate=pl.CostEstimate(flops=4 * rows * wide * units, transcendentals=rows * units, bytes_accessed=w.size * 2),
        name="hidden",
    )(at, x, w, w)


def own_body(at_ref, w_ref, hidden_ref, cols_ref, out_ref, buf, sem):
    part = buf.shape[0]
    copy = pltpu.make_async_copy(w_ref.at[pl.ds(at_ref[0] * part, part), 2], buf, sem)
    copy.start()
    copy.wait()
    out_ref[...] = cols_ref[...] + 0.5 * dot(hidden_ref[...], buf[...].reshape(-1, buf.shape[2]), 1, 1)


def own_part(at, hidden, w, cols, n):
    spread, _, deep, units = w.shape
    rows, share = cols.shape
    vmem = pl.BlockSpec(memory_space=pltpu.VMEM)
    return pl.pallas_call(
        own_body,
        out_shape=jax.ShapeDtypeStruct((rows, share), f32),
        in_specs=[pl.BlockSpec(memory_space=pltpu.SMEM), pl.BlockSpec(memory_space=pltpu.HBM), vmem, vmem],
        out_specs=vmem,
        scratch_shapes=[pltpu.VMEM((spread // n, deep, units), bf16), pltpu.SemaphoreType.DMA],
        compiler_params=pltpu.CompilerParams(vmem_limit_bytes=8 * MIB),
        cost_estimate=pl.CostEstimate(flops=2 * rows * share * units, transcendentals=0, bytes_accessed=2 * share * units),
        name="own",
    )(at, w, hidden, cols)


def sides_body(n, at_ref, w_ref, hidden_ref, low_ref, high_ref, up_ref, down_ref, buf, sem):
    part = buf.shape[1]
    half = low_ref.shape[0]
    copies = []
    for i, k in enumerate((1, n - 1)):
        j = (at_ref[0] + k) % n
        copies.append(pltpu.make_async_copy(w_ref.at[pl.ds(j * part, part), 2], buf.at[i], sem.at[i]))
        copies[i].start()
    copies[0].wait()
    piece = dot(hidden_ref[...], buf[0].reshape(-1, buf.shape[3]), 1, 1)
    up_ref[:half] = (piece[:half] + low_ref[...].astype(f32)).astype(bf16)
    up_ref[half:] = piece[half:].astype(bf16)
    copies[1].wait()
    piece = dot(hidden_ref[...], buf[1].reshape(-1, buf.shape[3]), 1, 1)
    down_ref[:half] = piece[:half].astype(bf16)
    down_ref[half:] = (piece[half:] + high_ref[...].astype(f32)).astype(bf16)


def side_parts(at, hidden, w, low, high, n):
    spread, _, deep, units = w.shape
    rows = hidden.shape[0]
    share = low.shape[1]
    vmem = pl.BlockSpec(memory_space=pltpu.VMEM)
    piece = jax.ShapeDtypeStruct((rows, share), bf16)
    return pl.pallas_call(
        functools.partial(sides_body, n),
        out_shape=(piece, piece),
        in_specs=[pl.BlockSpec(memory_space=pltpu.SMEM), pl.BlockSpec(memory_space=pltpu.HBM), vmem, vmem, vmem],
        out_specs=(vmem, vmem),
        scratch_shapes=[pltpu.VMEM((2, spread // n, deep, units), bf16), pltpu.SemaphoreType.DMA((2,))],
        compiler_params=pltpu.CompilerParams(vmem_limit_bytes=12 * MIB),
        cost_estimate=pl.CostEstimate(flops=4 * rows * share * units, transcendentals=0, bytes_accessed=4 * share * units),
        name="sides",
    )(at, w, hidden, low, high)


def local(
    residual,
    queries_a,
    keys_a,
    values_a,
    queries_b,
    keys_b,
    values_b,
    mix_lambda,
    head_gain,
    out_a,
    out_b,
    norm_gain,
    w_gate,
    w_up,
    w_down,
):
    wa = queries_a.shape[1] // 2
    wb = queries_b.shape[1] // 2
    vd = values_a.shape[1]
    consts = (wa**-0.5 * log2e, wb**-0.5 * log2e)
    n = lax.axis_size("tp")
    share = residual.shape[1] // n
    at = lax.axis_index("tp").astype(jnp.int32)[None]
    at, keys_a = lax.optimization_barrier((at, keys_a))

    kv, q = pack(((keys_a, keys_b, values_a, values_b), 1), ((queries_a, queries_b), 1))
    near = [kv, along_z(kv, 1), None, along_z(kv, 3)]
    queries = [q] + [along_y(q, k) for k in range(1, 4)]
    kv_far = other_core(kv)
    (oo,) = pack(((out_a, out_b), 0))
    outs = [oo] + [along_x(oo, k) for k in range(1, 4)]
    (three,) = pack(((w_gate, w_up, w_down.T), 0))
    three, queries[1], queries[3] = lax.optimization_barrier((three, queries[1], queries[3]))
    weights = lax.all_gather(three, "sp", axis=0, tiled=True)
    weights = in_hbm(weights.reshape(-1, 3, *w_gate.shape))
    kv, queries[1] = lax.optimization_barrier((kv, queries[1]))
    near[2] = along_z(kv, 2)

    go = functools.partial(attend, consts=consts, wa=wa, wb=wb, vd=vd)
    pairs = [[queries[k] for k in g] for g in ((2, 1), (3, 0))]
    state = go(pairs, [kv, kv_far], None, None)
    one, three, *state = lax.optimization_barrier((near[1], near[3], *state))
    far = {1: other_core(one), 3: other_core(three)}
    state = go(pairs, [one, three], state, None)
    two, *state = lax.optimization_barrier((near[2], *state))
    last = [far[1], far[3], two, other_core(two)]
    back = {}
    back[2], back[1] = go([[queries[2], queries[1]]], last, state, (0, 0, True))
    (back[3],) = go([[queries[3]]], last, state, (1, 0, True))
    back = {k: along_y(back[k], -k) for k in (2, 1, 3)}
    own = go([[queries[0]]], last, state, (1, 1, False))
    heads = merge(own, [back[k] for k in (1, 3, 2)], mix_lambda, head_gain, consts, vd)

    everyone = [heads] + [along_x(heads, k) for k in range(1, 4)]
    normed, cols = project(at, everyone, outs, residual, norm_gain[None], share)
    hidden, low, high = hidden_of(at, normed, weights, n)
    low, high = along_x(low, 1), along_x(high, -1)
    mine = own_part(at, hidden, weights, cols, n)
    up, down = side_parts(at, hidden, weights, low, high, n)
    arrived = along_x(up, 1).astype(f32) + along_x(down, -1).astype(f32)
    return (mine + 0.5 * arrived).astype(bf16)


def solution(mesh):
    in_specs = (
        P("sp", None),
        P("sp", "tp"),
        P("sp", "tp"),
        P("sp", "tp"),
        P("sp", "tp"),
        P("sp", "tp"),
        P("sp", "tp"),
        P(None, "tp"),
        P(),
        P("tp", None),
        P("tp", None),
        P(),
        P("sp", "tp"),
        P("sp", "tp"),
        P("tp", "sp"),
    )
    out_specs = P("sp", "tp")

    return jax.shard_map(local, mesh=mesh, in_specs=in_specs, out_specs=out_specs, check_vma=False)
```

profile of v0, /device:TPU:14, one launch (start us, length us, event | category | flops | bytes accessed | tf_op | source)
XLA Modules:
  0.0 171.6 jit_solution(12899768523496198398)
XLA Ops:
  7.8 1.6 collective-permute-start
  9.9 1.9 %pack.3 = bf16[192,1408]{1,0:T(8,128)(2,1)} custom-call(bf16[64,1408]{1,0:T(8,128)(2,1)} %refs_0_.2, bf16[64,1408]{1,0:T(8,128)(2,1)} %refs_1_.3, bf16[64,1408]{1,0:T(8,128)(2,1)} %bitcast.11), custom_call_target="tpu_custom_call" | custom-call | tf_op jit(solution)/shard_map/pack/pallas_call | solution.py:73
  11.8 4.8 %collective-permute-done.refs_1_ = bf16[384,384]{1,0:T(8,128)(2,1)S(1)} collective-permute-done((bf16[384,384]{1,0:T(8,128)(2,1)S(1)}, bf16[384,384]{1,0:T(8,128)(2,1)S(1)}, u32[]{:S(2)}, u32[]{:S(2)}) %collective-permute-start) | collective-permute-done | bytes 294944 | tf_op jit(solution)/shard_map/ppermute | solution.py:24
  18.0 2.4 %collective-permute-start.4 = (bf16[384,384]{1,0:T(8,128)(2,1)S(1)}, bf16[384,384]{1,0:T(8,128)(2,1)S(1)}, u32[]{:S(2)}, u32[]{:S(2)}) collective-permute-start(bf16[384,384]{1,0:T(8,128)(2,1)S(1)} %get-tuple-element.38.refs_3_.refs_0_), channel_id=1, source_target_pairs={{0,16},{4,20},{8,24},{12,28},{16,0},{20,4},{24,8},{28,12},{32,48},... | collective-permute-start | bytes 884744 | tf_op jit(solution)/shard_map/ppermute | solution.py:24
  20.4 1.9 %collective-permute-start.2 = (bf16[384,640]{1,0:T(8,128)(2,1)S(1)}, bf16[384,640]{1,0:T(8,128)(2,1)S(1)}, u32[]{:S(2)}, u32[]{:S(2)}) collective-permute-start(bf16[384,640]{1,0:T(8,128)(2,1)S(1)} %get-tuple-element.44.refs_4_), channel_id=1, source_target_pairs={{0,32},{4,36},{8,40},{12,44},{16,48},{20,52},{24,56},{28,60},{32,6... | collective-permute-start | bytes 1474568 | tf_op jit(solution)/shard_map/ppermute | solution.py:28
  22.3 2.1 %collective-permute-start.3 = (bf16[384,640]{1,0:T(8,128)(2,1)S(1)}, bf16[384,640]{1,0:T(8,128)(2,1)S(1)}, u32[]{:S(2)}, u32[]{:S(2)}) collective-permute-start(bf16[384,640]{1,0:T(8,128)(2,1)S(1)} %get-tuple-element.44.refs_4_), channel_id=1, source_target_pairs={{0,96},{4,100},{8,104},{12,108},{16,112},{20,116},{24,120},{28,124... | collective-permute-start | bytes 1474568 | tf_op jit(solution)/shard_map/ppermute | solution.py:28
  24.5 1.9 %collective-permute-start.8 = (bf16[384,640]{1,0:T(8,128)(2,1)S(1)}, bf16[384,640]{1,0:T(8,128)(2,1)S(1)}, u32[]{:S(2)}, u32[]{:S(2)}) collective-permute-start(bf16[384,640]{1,0:T(8,128)(2,1)S(1)} %get-tuple-element.44.refs_4_), channel_id=1, source_target_pairs={{0,64},{4,68},{8,72},{12,76},{16,80},{20,84},{24,88},{28,92},{32,9... | collective-permute-start | bytes 1474568 | tf_op jit(solution)/shard_map/ppermute | solution.py:28
  26.3 2.6 %collective-permute-done.4.refs_0_ = bf16[384,384]{1,0:T(8,128)(2,1)S(1)} collective-permute-done((bf16[384,384]{1,0:T(8,128)(2,1)S(1)}, bf16[384,384]{1,0:T(8,128)(2,1)S(1)}, u32[]{:S(2)}, u32[]{:S(2)}) %collective-permute-start.4) | collective-permute-done | bytes 294944 | tf_op jit(solution)/shard_map/ppermute | solution.py:24
  29.0 8.1 %attend.5 = (f32[2,512,768]{2,1,0:T(8,128)S(1)}, f32[2,16,768]{2,1,0:T(8,128)S(1)}) custom-call(bf16[384,384]{1,0:T(8,128)(2,1)S(1)} %collective-permute-done.4.refs_0_, bf16[384,384]{1,0:T(8,128)(2,1)S(1)} %collective-permute-done.refs_1_, bf16[384,384]{1,0:T(8,128)(2,1)S(1)} %collective-permute-done.1.refs_2_.refs_0_, ...), custom_call_target="tpu_custom_call" | custom-call | flops 2415919104 | bytes 983040 | tf_op jit(solution)/shard_map/attend/pallas_call | solution.py:250
  37.9 4.6 %collective-permute-done.3.refs_5_ = bf16[384,640]{1,0:T(8,128)(2,1)S(1)} collective-permute-done((bf16[384,640]{1,0:T(8,128)(2,1)S(1)}, bf16[384,640]{1,0:T(8,128)(2,1)S(1)}, u32[]{:S(2)}, u32[]{:S(2)}) %collective-permute-start.3) | collective-permute-done | bytes 491552 | tf_op jit(solution)/shard_map/ppermute | solution.py:28
  42.9 8.2 %attend.6 = (f32[2,512,768]{2,1,0:T(8,128)S(1)}, f32[2,16,768]{2,1,0:T(8,128)S(1)}) custom-call(bf16[384,384]{1,0:T(8,128)(2,1)S(1)} %collective-permute-done.4.refs_0_, bf16[384,384]{1,0:T(8,128)(2,1)S(1)} %collective-permute-done.refs_1_, bf16[384,384]{1,0:T(8,128)(2,1)S(1)} %collective-permute-done.1.refs_2_.refs_0_, ...), custom_call_target="tpu_custom_call" | custom-call | flops 2415919104 | bytes 983040 | tf_op jit(solution)/shard_map/attend/pallas_call | solution.py:250
  51.1 5.2 %collective-permute-done.8.refs_3_.refs_4_ = bf16[384,640]{1,0:T(8,128)(2,1)S(1)} collective-permute-done((bf16[384,640]{1,0:T(8,128)(2,1)S(1)}, bf16[384,640]{1,0:T(8,128)(2,1)S(1)}, u32[]{:S(2)}, u32[]{:S(2)}) %collective-permute-start.8) | collective-permute-done | bytes 491552 | tf_op jit(solution)/shard_map/ppermute | solution.py:28
  58.1 2.4 %collective-permute-start.17 = (bf16[256,2048]{1,0:T(8,128)(2,1)S(1)}, bf16[256,2048]{1,0:T(8,128)(2,1)S(1)}, u32[]{:S(2)}, u32[]{:S(2)}) collective-permute-start(bf16[256,2048]{1,0:T(8,128)(2,1)S(1)} %pack.5.refs_5_), channel_id=1, source_target_pairs={{0,2},{1,3},{2,0},{3,1},{4,6},{5,7},{6,4},{7,5},{8,10},{9,11},{10,... | collective-permute-start | bytes 3145736 | tf_op jit(solution)/shard_map/ppermute | solution.py:36
  60.6 5.4 %attend.9 = bf16[544,384]{1,0:T(8,128)(2,1)S(1)} custom-call(bf16[384,384]{1,0:T(8,128)(2,1)S(1)} %collective-permute-done.1.refs_2_.refs_0_, bf16[384,640]{1,0:T(8,128)(2,1)S(1)} %collective-permute-done.6.refs_1_.refs_2_, bf16[384,640]{1,0:T(8,128)(2,1)S(1)} %collective-permute-done.7.refs_2_.refs_3_, ...), custom_call_target="tpu_custom_call" | custom-call | flops 1207959552 | bytes 1966080 | tf_op jit(solution)/shard_map/attend/pallas_call | solution.py:250
  66.1 8.9 %attend.8 = (bf16[544,384]{1,0:T(8,128)(2,1)S(1)}, bf16[544,384]{1,0:T(8,128)(2,1)S(1)}) custom-call(bf16[384,384]{1,0:T(8,128)(2,1)S(1)} %collective-permute-done.4.refs_0_, bf16[384,384]{1,0:T(8,128)(2,1)S(1)} %collective-permute-done.refs_1_, bf16[384,640]{1,0:T(8,128)(2,1)S(1)} %collective-permute-done.6.refs_1_.refs_2_, ...), custom_call_target="tpu_custom_call" | custom-call | flops 2415919104 | bytes 1966080 | tf_op jit(solution)/shard_map/attend/pallas_call | solution.py:250
  75.1 2.1 %collective-permute-start.10 = (bf16[544,384]{1,0:T(8,128)(2,1)S(1)}, bf16[544,384]{1,0:T(8,128)(2,1)S(1)}, u32[]{:S(2)}, u32[]{:S(2)}) collective-permute-start(bf16[544,384]{1,0:T(8,128)(2,1)S(1)} %get-tuple-element.58), channel_id=1, source_target_pairs={{0,24},{4,28},{8,0},{12,4},{16,8},{20,12},{24,16},{28,20},{32,56},... | collective-permute-start | bytes 1253384 | tf_op jit(solution)/shard_map/ppermute | solution.py:24
  77.2 10.1 %collective-permute-done.11.refs_1_ = bf16[544,384]{1,0:T(8,128)(2,1)S(1)} collective-permute-done((bf16[544,384]{1,0:T(8,128)(2,1)S(1)}, bf16[544,384]{1,0:T(8,128)(2,1)S(1)}, u32[]{:S(2)}, u32[]{:S(2)}) %collective-permute-start.11) | collective-permute-done | bytes 417824 | tf_op jit(solution)/shard_map/ppermute | solution.py:24
  88.5 5.4 %attend.7 = (f32[1,512,384]{2,1,0:T(8,128)S(1)}, f32[1,16,384]{2,1,0:T(8,128)S(1)}) custom-call(bf16[384,384]{1,0:T(8,128)(2,1)S(1)} %get-tuple-element.38.refs_3_.refs_0_, bf16[384,640]{1,0:T(8,128)(2,1)S(1)} %collective-permute-done.6.refs_1_.refs_2_, bf16[384,640]{1,0:T(8,128)(2,1)S(1)} %collective-permute-done.7.refs_2_.refs_3_, ...), custom_call_target="tpu_custom_call" | custom-call | flops 1207959552 | bytes 1966080 | tf_op jit(solution)/shard_map/attend/pallas_call | solution.py:250
  93.9 2.4 %collective-permute-done.10.refs_0_ = bf16[544,384]{1,0:T(8,128)(2,1)S(1)} collective-permute-done((bf16[544,384]{1,0:T(8,128)(2,1)S(1)}, bf16[544,384]{1,0:T(8,128)(2,1)S(1)}, u32[]{:S(2)}, u32[]{:S(2)}) %collective-permute-start.10) | collective-permute-done | bytes 417824 | tf_op jit(solution)/shard_map/ppermute | solution.py:24
  96.3 19.1 %collective-permute-done.12.refs_2_ = bf16[544,384]{1,0:T(8,128)(2,1)S(1)} collective-permute-done((bf16[544,384]{1,0:T(8,128)(2,1)S(1)}, bf16[544,384]{1,0:T(8,128)(2,1)S(1)}, u32[]{:S(2)}, u32[]{:S(2)}) %collective-permute-start.12) | collective-permute-done | bytes 417824 | tf_op jit(solution)/shard_map/ppermute | solution.py:24
  116.0 3.2 %collective-permute-start.13 = (bf16[384,256]{1,0:T(8,128)(2,1)S(1)}, bf16[384,256]{1,0:T(8,128)(2,1)S(1)}, u32[]{:S(2)}, u32[]{:S(2)}) collective-permute-start(bf16[384,256]{1,0:T(8,128)(2,1)S(1)} %merge.1.refs_1_), channel_id=1, source_target_pairs={{0,1},{1,2},{2,3},{3,0},{4,5},{5,6},{6,7},{7,4},{8,9},{9,10},{10,1... | collective-permute-start | bytes 589832 | tf_op jit(solution)/shard_map/ppermute | solution.py:36
  120.6 5.9 %collective-permute-done.13.refs_2_ = bf16[384,256]{1,0:T(8,128)(2,1)S(1)} collective-permute-done((bf16[384,256]{1,0:T(8,128)(2,1)S(1)}, bf16[384,256]{1,0:T(8,128)(2,1)S(1)}, u32[]{:S(2)}, u32[]{:S(2)}) %collective-permute-start.13) | collective-permute-done | bytes 196640 | tf_op jit(solution)/shard_map/ppermute | solution.py:36
  126.5 1.6 collective-permute-done.14.refs_3_
  128.2 1.9 %collective-permute-done.15.refs_4_ = bf16[384,256]{1,0:T(8,128)(2,1)S(1)} collective-permute-done((bf16[384,256]{1,0:T(8,128)(2,1)S(1)}, bf16[384,256]{1,0:T(8,128)(2,1)S(1)}, u32[]{:S(2)}, u32[]{:S(2)}) %collective-permute-start.15) | collective-permute-done | bytes 196640 | tf_op jit(solution)/shard_map/ppermute | solution.py:36
  130.0 2.4 %project.1 = (bf16[384,2048]{1,0:T(8,128)(2,1)S(1)}, f32[384,512]{1,0:T(8,128)S(1)}) custom-call(s32[1]{0:T(128)} %bitcast.refs_0_.at_ref, bf16[384,256]{1,0:T(8,128)(2,1)S(1)} %merge.1.refs_1_, bf16[384,256]{1,0:T(8,128)(2,1)S(1)} %collective-permute-done.13.refs_2_, bf16[384,256]{1,0:T(8,128)(2,1)S(1)} %collective-permute-done.14.refs_3_, ...), custom_call_target="tpu_custom_call" | custom-call | flops 1610612736 | bytes 8388608 | tf_op jit(solution)/shard_map/project/pallas_call | solution.py:316
  132.5 9.8 %hidden.1 = (bf16[384,1408]{1,0:T(8,128)(2,1)S(1)}, bf16[192,512]{1,0:T(8,128)(2,1)S(1)}, bf16[192,512]{1,0:T(8,128)(2,1)S(1)}) custom-call(s32[1]{0:T(128)} %bitcast.refs_0_.at_ref, bf16[384,2048]{1,0:T(8,128)(2,1)S(1)} %get-tuple-element.60.x_ref, bf16[32,3,64,1408]{3,2,1,0:T(8,128)(2,1)} %bitcast.7, bf16[32,3,64,1408]{3,2,1,0:T(8,128)(2,1)} %bitcast.8), custom_call_target="tpu_custom_call" | custom-call | flops 4429185024 | bytes 17301504 | tf_op jit(solution)/shard_map/hidden/pallas_call | solution.py:361
  144.4 4.5 %collective-permute-done.19.low_ref = bf16[192,512]{1,0:T(8,128)(2,1)S(1)} collective-permute-done((bf16[192,512]{1,0:T(8,128)(2,1)S(1)}, bf16[192,512]{1,0:T(8,128)(2,1)S(1)}, u32[]{:S(2)}, u32[]{:S(2)}) %collective-permute-start.19) | collective-permute-done | bytes 196640 | tf_op jit(solution)/shard_map/ppermute | solution.py:36
  150.2 3.0 %sides.1 = (bf16[384,512]{1,0:T(8,128)(2,1)S(1)}, bf16[384,512]{1,0:T(8,128)(2,1)S(1)}) custom-call(s32[1]{0:T(128)} %bitcast.refs_0_.at_ref, bf16[32,3,64,1408]{3,2,1,0:T(8,128)(2,1)} %bitcast.9, bf16[384,1408]{1,0:T(8,128)(2,1)S(1)} %get-tuple-element.61.hidden_ref, bf16[192,512]{1,0:T(8,128)(2,1)S(1)} %collective-permute-done.19.low_ref, ...), custom_call_target="tpu_custom_call" | custom-call | flops 1107296256 | bytes 2883584 | tf_op jit(solution)/shard_map/sides/pallas_call | solution.py:437
  153.5 1.8 %collective-permute-start.22 = (bf16[384,512]{1,0:T(8,128)(2,1)S(1)}, bf16[384,512]{1,0:T(8,128)(2,1)S(1)}, u32[]{:S(2)}, u32[]{:S(2)}) collective-permute-start(bf16[384,512]{1,0:T(8,128)(2,1)S(1)} %get-tuple-element.66), channel_id=1, source_target_pairs={{0,3},{1,0},{2,1},{3,2},{4,7},{5,4},{6,5},{7,6},{8,11},{9,8},{10,9... | collective-permute-start | bytes 1179656 | tf_op jit(solution)/shard_map/ppermute | solution.py:36
  155.3 2.2 %own.1 = f32[384,512]{1,0:T(8,128)S(1)} custom-call(s32[1]{0:T(128)} %bitcast.refs_0_.at_ref, bf16[32,3,64,1408]{3,2,1,0:T(8,128)(2,1)} %bitcast.10, bf16[384,1408]{1,0:T(8,128)(2,1)S(1)} %get-tuple-element.61.hidden_ref, f32[384,512]{1,0:T(8,128)S(1)} %get-tuple-element.62.cols_ref), custom_call_target="tpu_custom_call" | custom-call | flops 553648128 | bytes 1441792 | tf_op jit(solution)/shard_map/own/pallas_call | solution.py:401
  157.5 5.0 %collective-permute-done.21 = bf16[384,512]{1,0:T(8,128)(2,1)S(1)} collective-permute-done((bf16[384,512]{1,0:T(8,128)(2,1)S(1)}, bf16[384,512]{1,0:T(8,128)(2,1)S(1)}, u32[]{:S(2)}, u32[]{:S(2)}) %collective-permute-start.21) | collective-permute-done | bytes 393248 | tf_op jit(solution)/shard_map/ppermute | solution.py:36
  162.4 1.3 collective-permute-done.22
  (39 shorter events, 14.2 us)
Async XLA Ops:
  6.5 125.9 %all-gather.2.cloned.1.call-start = ((), (), s32[]{:S(2)}) async-start(), calls=%async_computation | async-start | bytes 17842176 | tf_op jit(solution)/shard_map/all_gather | solution.py:483
  7.8 8.8 %collective-permute-start = (bf16[384,384]{1,0:T(8,128)(2,1)S(1)}, bf16[384,384]{1,0:T(8,128)(2,1)S(1)}, u32[]{:S(2)}, u32[]{:S(2)}) collective-permute-start(bf16[384,384]{1,0:T(8,128)(2,1)S(1)} %get-tuple-element.38.refs_3_.refs_0_), channel_id=1, source_target_pairs={{0,8},{4,12},{8,16},{12,20},{16,24},{20,28},{24,0},{28,4},{32,40},... | collective-permute-start | bytes 884744 | tf_op jit(solution)/shard_map/ppermute | solution.py:24
  9.5 8.5 %collective-permute-start.1 = (bf16[384,384]{1,0:T(8,128)(2,1)S(1)}, bf16[384,384]{1,0:T(8,128)(2,1)S(1)}, u32[]{:S(2)}, u32[]{:S(2)}) collective-permute-start(bf16[384,384]{1,0:T(8,128)(2,1)S(1)} %get-tuple-element.38.refs_3_.refs_0_), channel_id=1, source_target_pairs={{0,24},{4,28},{8,0},{12,4},{16,8},{20,12},{24,16},{28,20},{32,56},... | collective-permute-start | bytes 884744 | tf_op jit(solution)/shard_map/ppermute | solution.py:24
  17.9 11.0 %collective-permute-start.5 = (bf16[384,640]{1,0:T(8,128)(2,1)S(1)}, bf16[384,640]{1,0:T(8,128)(2,1)S(1)}, u32[]{:S(2)}, u32[]{:S(2)}) collective-permute-start(bf16[384,640]{1,0:T(8,128)(2,1)S(1)} %get-tuple-element.44.refs_4_), channel_id=1, source_target_pairs={{0,4},{4,0},{8,12},{12,8},{16,20},{20,16},{24,28},{28,24},{32,36},... | collective-permute-start | bytes 1474568 | tf_op jit(solution)/shard_map/ppermute | solution.py:32
  18.0 10.9 %collective-permute-start.4 = (bf16[384,384]{1,0:T(8,128)(2,1)S(1)}, bf16[384,384]{1,0:T(8,128)(2,1)S(1)}, u32[]{:S(2)}, u32[]{:S(2)}) collective-permute-start(bf16[384,384]{1,0:T(8,128)(2,1)S(1)} %get-tuple-element.38.refs_3_.refs_0_), channel_id=1, source_target_pairs={{0,16},{4,20},{8,24},{12,28},{16,0},{20,4},{24,8},{28,12},{32,48},... | collective-permute-start | bytes 884744 | tf_op jit(solution)/shard_map/ppermute | solution.py:24
  20.4 17.4 %collective-permute-start.2 = (bf16[384,640]{1,0:T(8,128)(2,1)S(1)}, bf16[384,640]{1,0:T(8,128)(2,1)S(1)}, u32[]{:S(2)}, u32[]{:S(2)}) collective-permute-start(bf16[384,640]{1,0:T(8,128)(2,1)S(1)} %get-tuple-element.44.refs_4_), channel_id=1, source_target_pairs={{0,32},{4,36},{8,40},{12,44},{16,48},{20,52},{24,56},{28,60},{32,6... | collective-permute-start | bytes 1474568 | tf_op jit(solution)/shard_map/ppermute | solution.py:28
  22.3 20.1 %collective-permute-start.3 = (bf16[384,640]{1,0:T(8,128)(2,1)S(1)}, bf16[384,640]{1,0:T(8,128)(2,1)S(1)}, u32[]{:S(2)}, u32[]{:S(2)}) collective-permute-start(bf16[384,640]{1,0:T(8,128)(2,1)S(1)} %get-tuple-element.44.refs_4_), channel_id=1, source_target_pairs={{0,96},{4,100},{8,104},{12,108},{16,112},{20,116},{24,120},{28,124... | collective-permute-start | bytes 1474568 | tf_op jit(solution)/shard_map/ppermute | solution.py:28
  24.5 31.9 %collective-permute-start.8 = (bf16[384,640]{1,0:T(8,128)(2,1)S(1)}, bf16[384,640]{1,0:T(8,128)(2,1)S(1)}, u32[]{:S(2)}, u32[]{:S(2)}) collective-permute-start(bf16[384,640]{1,0:T(8,128)(2,1)S(1)} %get-tuple-element.44.refs_4_), channel_id=1, source_target_pairs={{0,64},{4,68},{8,72},{12,76},{16,80},{20,84},{24,88},{28,92},{32,9... | collective-permute-start | bytes 1474568 | tf_op jit(solution)/shard_map/ppermute | solution.py:28
  42.4 18.2 %collective-permute-start.6 = (bf16[384,640]{1,0:T(8,128)(2,1)S(1)}, bf16[384,640]{1,0:T(8,128)(2,1)S(1)}, u32[]{:S(2)}, u32[]{:S(2)}) collective-permute-start(bf16[384,640]{1,0:T(8,128)(2,1)S(1)} %collective-permute-done.2.refs_4_), channel_id=1, source_target_pairs={{0,4},{4,0},{8,12},{12,8},{16,20},{20,16},{24,28},{28,24},{32,36},... | collective-permute-start | bytes 1474568 | tf_op jit(solution)/shard_map/ppermute | solution.py:32
  42.4 18.2 %collective-permute-start.7 = (bf16[384,640]{1,0:T(8,128)(2,1)S(1)}, bf16[384,640]{1,0:T(8,128)(2,1)S(1)}, u32[]{:S(2)}, u32[]{:S(2)}) collective-permute-start(bf16[384,640]{1,0:T(8,128)(2,1)S(1)} %collective-permute-done.3.refs_5_), channel_id=1, source_target_pairs={{0,4},{4,0},{8,12},{12,8},{16,20},{20,16},{24,28},{28,24},{32,36},... | collective-permute-start | bytes 1474568 | tf_op jit(solution)/shard_map/ppermute | solution.py:32
  56.4 4.2 %collective-permute-start.9 = (bf16[384,640]{1,0:T(8,128)(2,1)S(1)}, bf16[384,640]{1,0:T(8,128)(2,1)S(1)}, u32[]{:S(2)}, u32[]{:S(2)}) collective-permute-start(bf16[384,640]{1,0:T(8,128)(2,1)S(1)} %collective-permute-done.8.refs_3_.refs_4_), channel_id=1, source_target_pairs={{0,4},{4,0},{8,12},{12,8},{16,20},{20,16},{24,28},{28,24},{32,36},... | collective-permute-start | bytes 1474568 | tf_op jit(solution)/shard_map/ppermute | solution.py:32
  57.6 61.7 %collective-permute-start.16 = (bf16[256,2048]{1,0:T(8,128)(2,1)S(1)}, bf16[256,2048]{1,0:T(8,128)(2,1)S(1)}, u32[]{:S(2)}, u32[]{:S(2)}) collective-permute-start(bf16[256,2048]{1,0:T(8,128)(2,1)S(1)} %pack.5.refs_5_), channel_id=1, source_target_pairs={{0,1},{1,2},{2,3},{3,0},{4,5},{5,6},{6,7},{7,4},{8,9},{9,10},{10,1... | collective-permute-start | bytes 3145736 | tf_op jit(solution)/shard_map/ppermute | solution.py:36
  58.1 62.5 %collective-permute-start.17 = (bf16[256,2048]{1,0:T(8,128)(2,1)S(1)}, bf16[256,2048]{1,0:T(8,128)(2,1)S(1)}, u32[]{:S(2)}, u32[]{:S(2)}) collective-permute-start(bf16[256,2048]{1,0:T(8,128)(2,1)S(1)} %pack.5.refs_5_), channel_id=1, source_target_pairs={{0,2},{1,3},{2,0},{3,1},{4,6},{5,7},{6,4},{7,5},{8,10},{9,11},{10,... | collective-permute-start | bytes 3145736 | tf_op jit(solution)/shard_map/ppermute | solution.py:36
  60.6 60.1 %collective-permute-start.18 = (bf16[256,2048]{1,0:T(8,128)(2,1)S(1)}, bf16[256,2048]{1,0:T(8,128)(2,1)S(1)}, u32[]{:S(2)}, u32[]{:S(2)}) collective-permute-start(bf16[256,2048]{1,0:T(8,128)(2,1)S(1)} %pack.5.refs_5_), channel_id=1, source_target_pairs={{0,3},{1,0},{2,1},{3,2},{4,7},{5,4},{6,5},{7,6},{8,11},{9,8},{10,9... | collective-permute-start | bytes 3145736 | tf_op jit(solution)/shard_map/ppermute | solution.py:36
  66.0 21.2 %collective-permute-start.11 = (bf16[544,384]{1,0:T(8,128)(2,1)S(1)}, bf16[544,384]{1,0:T(8,128)(2,1)S(1)}, u32[]{:S(2)}, u32[]{:S(2)}) collective-permute-start(bf16[544,384]{1,0:T(8,128)(2,1)S(1)} %attend.9), channel_id=1, source_target_pairs={{0,8},{4,12},{8,16},{12,20},{16,24},{20,28},{24,0},{28,4},{32,40},... | collective-permute-start | bytes 1253384 | tf_op jit(solution)/shard_map/ppermute | solution.py:24
  75.1 40.4 %copy-start.2 = (f32[2,128]{1,0:T(2,128)S(1)}, f32[2,128]{1,0:T(2,128)}, u32[]{:S(2)}) copy-start(f32[2,128]{1,0:T(2,128)} %gain_ref.1) | copy-start | bytes 3076
  75.1 40.4 %copy-start.3 = (f32[2,1]{0,1:T(1,128)S(1)}, f32[2,1]{0,1:T(1,128)}, u32[]{:S(2)}) copy-start(f32[2,1]{0,1:T(1,128)} %param.22) | copy-start | bytes 28
  75.1 21.2 %collective-permute-start.10 = (bf16[544,384]{1,0:T(8,128)(2,1)S(1)}, bf16[544,384]{1,0:T(8,128)(2,1)S(1)}, u32[]{:S(2)}, u32[]{:S(2)}) collective-permute-start(bf16[544,384]{1,0:T(8,128)(2,1)S(1)} %get-tuple-element.58), channel_id=1, source_target_pairs={{0,24},{4,28},{8,0},{12,4},{16,8},{20,12},{24,16},{28,20},{32,56},... | collective-permute-start | bytes 1253384 | tf_op jit(solution)/shard_map/ppermute | solution.py:24
  87.3 42.8 %copy-start = (bf16[384,2048]{1,0:T(8,128)(2,1)S(1)}, bf16[384,2048]{1,0:T(8,128)(2,1)}, u32[]{:S(2)}) copy-start(bf16[384,2048]{1,0:T(8,128)(2,1)} %refs_9_.1) | copy-start | bytes 4718596
  87.3 42.8 %copy-start.1 = (f32[2048]{0:T(1024)S(1)}, f32[2048]{0:T(1024)}, u32[]{:S(2)}) copy-start(f32[2048]{0:T(1024)} %param.26) | copy-start | bytes 24580
  87.3 28.1 %collective-permute-start.12 = (bf16[544,384]{1,0:T(8,128)(2,1)S(1)}, bf16[544,384]{1,0:T(8,128)(2,1)S(1)}, u32[]{:S(2)}, u32[]{:S(2)}) collective-permute-start(bf16[544,384]{1,0:T(8,128)(2,1)S(1)} %get-tuple-element.59), channel_id=1, source_target_pairs={{0,16},{4,20},{8,24},{12,28},{16,0},{20,4},{24,8},{28,12},{32,48},... | collective-permute-start | bytes 1253384 | tf_op jit(solution)/shard_map/ppermute | solution.py:24
  116.0 10.5 %collective-permute-start.13 = (bf16[384,256]{1,0:T(8,128)(2,1)S(1)}, bf16[384,256]{1,0:T(8,128)(2,1)S(1)}, u32[]{:S(2)}, u32[]{:S(2)}) collective-permute-start(bf16[384,256]{1,0:T(8,128)(2,1)S(1)} %merge.1.refs_1_), channel_id=1, source_target_pairs={{0,1},{1,2},{2,3},{3,0},{4,5},{5,6},{6,7},{7,4},{8,9},{9,10},{10,1... | collective-permute-start | bytes 589832 | tf_op jit(solution)/shard_map/ppermute | solution.py:36
  119.2 9.0 %collective-permute-start.14 = (bf16[384,256]{1,0:T(8,128)(2,1)S(1)}, bf16[384,256]{1,0:T(8,128)(2,1)S(1)}, u32[]{:S(2)}, u32[]{:S(2)}) collective-permute-start(bf16[384,256]{1,0:T(8,128)(2,1)S(1)} %merge.1.refs_1_), channel_id=1, source_target_pairs={{0,2},{1,3},{2,0},{3,1},{4,6},{5,7},{6,4},{7,5},{8,10},{9,11},{10,... | collective-permute-start | bytes 589832 | tf_op jit(solution)/shard_map/ppermute | solution.py:36
  119.3 10.7 %collective-permute-start.15 = (bf16[384,256]{1,0:T(8,128)(2,1)S(1)}, bf16[384,256]{1,0:T(8,128)(2,1)S(1)}, u32[]{:S(2)}, u32[]{:S(2)}) collective-permute-start(bf16[384,256]{1,0:T(8,128)(2,1)S(1)} %merge.1.refs_1_), channel_id=1, source_target_pairs={{0,3},{1,0},{2,1},{3,2},{4,7},{5,4},{6,5},{7,6},{8,11},{9,8},{10,9... | collective-permute-start | bytes 589832 | tf_op jit(solution)/shard_map/ppermute | solution.py:36
  142.3 6.6 %collective-permute-start.19 = (bf16[192,512]{1,0:T(8,128)(2,1)S(1)}, bf16[192,512]{1,0:T(8,128)(2,1)S(1)}, u32[]{:S(2)}, u32[]{:S(2)}) collective-permute-start(bf16[192,512]{1,0:T(8,128)(2,1)S(1)} %get-tuple-element.63), channel_id=1, source_target_pairs={{0,1},{1,2},{2,3},{3,0},{4,5},{5,6},{6,7},{7,4},{8,9},{9,10},{10,1... | collective-permute-start | bytes 589832 | tf_op jit(solution)/shard_map/ppermute | solution.py:36
  143.1 7.1 %collective-permute-start.20 = (bf16[192,512]{1,0:T(8,128)(2,1)S(1)}, bf16[192,512]{1,0:T(8,128)(2,1)S(1)}, u32[]{:S(2)}, u32[]{:S(2)}) collective-permute-start(bf16[192,512]{1,0:T(8,128)(2,1)S(1)} %get-tuple-element.64), channel_id=1, source_target_pairs={{0,3},{1,0},{2,1},{3,2},{4,7},{5,4},{6,5},{7,6},{8,11},{9,8},{10,9... | collective-permute-start | bytes 589832 | tf_op jit(solution)/shard_map/ppermute | solution.py:36
  153.2 9.3 %collective-permute-start.21 = (bf16[384,512]{1,0:T(8,128)(2,1)S(1)}, bf16[384,512]{1,0:T(8,128)(2,1)S(1)}, u32[]{:S(2)}, u32[]{:S(2)}) collective-permute-start(bf16[384,512]{1,0:T(8,128)(2,1)S(1)} %get-tuple-element.65), channel_id=1, source_target_pairs={{0,1},{1,2},{2,3},{3,0},{4,5},{5,6},{6,7},{7,4},{8,9},{9,10},{10,1... | collective-permute-start | bytes 1179656 | tf_op jit(solution)/shard_map/ppermute | solution.py:36
  153.5 10.3 %collective-permute-start.22 = (bf16[384,512]{1,0:T(8,128)(2,1)S(1)}, bf16[384,512]{1,0:T(8,128)(2,1)S(1)}, u32[]{:S(2)}, u32[]{:S(2)}) collective-permute-start(bf16[384,512]{1,0:T(8,128)(2,1)S(1)} %get-tuple-element.66), channel_id=1, source_target_pairs={{0,3},{1,0},{2,1},{3,2},{4,7},{5,4},{6,5},{7,6},{8,11},{9,8},{10,9... | collective-permute-start | bytes 1179656 | tf_op jit(solution)/shard_map/ppermute | solution.py:36
Sparse Core Ops, SparseCore 0:
  18.1 101.6 all-gather.1
where the time goes:
time: 172 us
  waiting for transfers between devices  72.5 us (42%)
  Pallas kernels  58.4 us (34%)
  starting transfers between devices  26.2 us (15%)
  between operations  13.6 us (8%)
    ppermute x6, waiting for transfers between devices, along_y(): lax.ppermute(x, 'sp', [(place(z, y, c), place(z, y + k, c)) for z, y, c i...  40.3 us
    pallas_call x5, Pallas kernels, attend(): pl.pallas_call(functools.partial(attend_body, groups, m, nk, state is not...  36.1 us
    ppermute x10, waiting for transfers between devices, along_x(): return lax.ppermute(x, 'tp', [(i, (i + k) % 4) for i in range(4)])  21.5 us
    ppermute x10, starting transfers between devices, along_x(): return lax.ppermute(x, 'tp', [(i, (i + k) % 4) for i in range(4)])  11.8 us
    ppermute x3, waiting for transfers between devices, along_z(): lax.ppermute(x, 'sp', [(place(z, y, c), place(z + k, y, c)) for z, y, c i...  10.6 us
    pallas_call x1, Pallas kernels, hidden_of(): pl.pallas_call(hidden_body, grid_spec=pltpu.PrefetchScalarGridSpec(num_sc...  9.78 us
    ppermute x6, starting transfers between devices, along_y(): lax.ppermute(x, 'sp', [(place(z, y, c), place(z, y + k, c)) for z, y, c i...  7.87 us
    ppermute x3, starting transfers between devices, along_z(): lax.ppermute(x, 'sp', [(place(z, y, c), place(z + k, y, c)) for z, y, c i...  5.9 us
  transfers between devices with their start and end apart: 24, of which 16 were waited for; matrix products, arithmetic and copies ran while one was open for 0% of the time, Pallas kernels for 26%

commit v1 on v0

--- a/solution.py
+++ b/solution.py
@@ -59,7 +59,7 @@
     return pltpu.with_memory_space_constraint(x, pltpu.HBM)
 
 
-def pack(*sides):
+def pack(*sides, fixed=True):
     layout, shapes = [], []
     for arrays, axis in sides:
         at, corners = 0, []
@@ -69,7 +69,7 @@
         other = arrays[0].shape[1 - axis]
         layout.append(corners)
         shapes.append(jax.ShapeDtypeStruct((at, other) if axis == 0 else (other, at), arrays[0].dtype))
-    flat = [in_hbm(a) for arrays, _ in sides for a in arrays]
+    flat = [in_hbm(a) if fixed else a for arrays, _ in sides for a in arrays]
     return pl.pallas_call(
         functools.partial(pack_body, layout),
         out_shape=tuple(shapes),
@@ -325,125 +325,135 @@
     )(at, *heads, *outs, residual, gain)
 
 
-CUTS = 2
-
-
-def hidden_body(at_ref, x_ref, w_ref, down_ref, hidden_ref, low_ref, high_ref, sum_ref):
-    step = pl.program_id(0)
-    spread, _, deep, units = w_ref.shape
-    tall = spread * deep
-    which, cut = step // CUTS, step % CUTS
-    more = dot(x_ref[:, pl.ds(pl.multiple_of(cut * tall, tall), tall)], w_ref[...].reshape(tall, units), 1, 0)
-
-    @pl.when(cut == 0)
-    def _():
-        sum_ref[which] = more
-
-    @pl.when(cut > 0)
-    def _():
-        sum_ref[which] = sum_ref[which] + more
-
-    @pl.when(step == 2 * CUTS - 1)
-    def _():
-        gate = sum_ref[0]
-        hidden_ref[...] = (gate / (1.0 + jnp.exp(-gate)) * sum_ref[1]).astype(bf16)
-        piece = dot(hidden_ref[...], down_ref[...].reshape(-1, units), 1, 1).astype(bf16)
-        half = piece.shape[0] // 2
-        low_ref[...] = piece[:half]
-        high_ref[...] = piece[half:]
-
-
-def hidden_of(at, x, w, n):
+def assemble_body(n, place_ref, *refs):
+    firsts, seconds, outs = refs[: 2 * n], refs[2 * n : 4 * n], refs[4 * n : 4 * n + 3]
+    sem = refs[4 * n + 3]
+    deep = outs[0].shape[1]
+    spot = place_ref[1]
+    y_here, z_here, core_here = (spot // 2) % 4, spot // 8, spot % 2
+    for c in range(2):
+        core = (core_here + c) % 2
+        for i in range(n):
+
+            def one(r, _):
+                to = ((z_here + 4 - i) % 4) * 8 + ((y_here + 4 - r) % 4) * 2 + core
+                first = firsts[c * n + i]
+                pltpu.make_async_copy(first.at[r, pl.ds(0, deep)], outs[0].at[to], sem.at[0]).start()
+                pltpu.make_async_copy(first.at[r, pl.ds(deep, deep)], outs[2].at[to], sem.at[2]).start()
+                to = ((z_here + 4 - r) % 4) * 8 + ((y_here + 4 - i) % 4) * 2 + core
+                pltpu.make_async_copy(seconds[c * n + i].at[r], outs[1].at[to], sem.at[1]).start()
+                return 0
+
+            lax.fori_loop(0, 4, one, 0)
+    for i in range(3):
+        pltpu.make_async_copy(outs[i], outs[i], sem.at[i]).wait()
+
+
+def assemble(place, firsts, seconds, n):
+    _, deep, units = seconds[0].shape
+    shape = jax.ShapeDtypeStruct((8 * n, deep, units), bf16)
+    vmem = pl.BlockSpec(memory_space=pltpu.VMEM)
+    return pl.pallas_call(
+        functools.partial(assemble_body, n),
+        out_shape=(shape,) * 3,
+        in_specs=[pl.BlockSpec(memory_space=pltpu.SMEM)] + [pl.BlockSpec(memory_space=pl.ANY)] * (4 * n),
+        out_specs=(vmem,) * 3,
+        scratch_shapes=[pltpu.SemaphoreType.DMA((3,))],
+        compiler_params=pltpu.CompilerParams(vmem_limit_bytes=20 * MIB),
+        name="assemble",
+    )(place, *firsts, *seconds)
+
+
+def product(hidden, down_ref, j, n):
+    part = down_ref.shape[0] // n
+    w = down_ref[pl.ds(j * part, part)].reshape(part * down_ref.shape[1], down_ref.shape[2])
+    return dot(hidden, w, 1, 1)
+
+
+LANES = 256
+
+
+def hidden_body(n, place_ref, x_ref, gate_ref, up_ref, down_ref, hidden_ref, low_ref, high_ref):
+    spread, deep, units = gate_ref.shape
+    full = units // LANES
+
+    def some(lanes, width):
+        gate = dot(x_ref[...], gate_ref[:, :, lanes].reshape(spread * deep, width), 1, 0)
+        up = dot(x_ref[...], up_ref[:, :, lanes].reshape(spread * deep, width), 1, 0)
+        hidden_ref[:, lanes] = (gate / (1.0 + jnp.exp(-gate)) * up).astype(bf16)
+
+    def one(i, _):
+        some(pl.ds(pl.multiple_of(i * LANES, LANES), LANES), LANES)
+        return 0
+
+    lax.fori_loop(0, full, one, 0)
+    if units % LANES:
+        some(slice(full * LANES, units), units % LANES)
+    piece = product(hidden_ref[...], down_ref, (place_ref[0] + 2) % n, n).astype(bf16)
+    half = piece.shape[0] // 2
+    low_ref[...] = piece[:half]
+    high_ref[...] = piece[half:]
+
+
+def hidden_of(place, x, gate, up, down, n):
     rows, wide = x.shape
-    spread, _, deep, units = w.shape
-    share = wide // n
-    whole = lambda p, at: (0, 0)
-    return pl.pallas_call(
-        hidden_body,
-        grid_spec=pltpu.PrefetchScalarGridSpec(
-            num_scalar_prefetch=1,
-            grid=(2 * CUTS,),
-            in_specs=[
-                pl.BlockSpec((rows, wide), whole),
-                pl.BlockSpec((spread // CUTS, 1, deep, units), lambda p, at: (p % CUTS, p // CUTS, 0, 0)),
-                pl.BlockSpec((spread // n, 1, deep, units), lambda p, at: ((at[0] + 2) % n, 2, 0, 0)),
-            ],
-            out_specs=(
-                pl.BlockSpec((rows, units), whole),
-                pl.BlockSpec((rows // 2, share), whole),
-                pl.BlockSpec((rows // 2, share), whole),
-            ),
-            scratch_shapes=[pltpu.VMEM((2, rows, units), f32)],
-        ),
-        out_shape=(
-            jax.ShapeDtypeStruct((rows, units), bf16),
-            jax.ShapeDtypeStruct((rows // 2, share), bf16),
-            jax.ShapeDtypeStruct((rows // 2, share), bf16),
-        ),
-        compiler_params=pltpu.CompilerParams(vmem_limit_bytes=36 * MIB, dimension_semantics=("arbitrary",)),
-        cost_estimate=pl.CostEstimate(flops=4 * rows * wide * units, transcendentals=rows * units, bytes_accessed=w.size * 2),
+    units = gate.shape[-1]
+    vmem = pl.BlockSpec(memory_space=pltpu.VMEM)
+    half = jax.ShapeDtypeStruct((rows // 2, wide // n), bf16)
+    return pl.pallas_call(
+        functools.partial(hidden_body, n),
+        out_shape=(jax.ShapeDtypeStruct((rows, units), bf16), half, half),
+        in_specs=[pl.BlockSpec(memory_space=pltpu.SMEM)] + [vmem] * 4,
+        out_specs=(vmem,) * 3,
+        compiler_params=pltpu.CompilerParams(vmem_limit_bytes=26 * MIB),
+        cost_estimate=pl.CostEstimate(flops=4 * rows * wide * units, transcendentals=rows * units, bytes_accessed=gate.size * 4),
         name="hidden",
-    )(at, x, w, w)
-
-
-def own_body(at_ref, w_ref, hidden_ref, cols_ref, out_ref, buf, sem):
-    part = buf.shape[0]
-    copy = pltpu.make_async_copy(w_ref.at[pl.ds(at_ref[0] * part, part), 2], buf, sem)
-    copy.start()
-    copy.wait()
-    out_ref[...] = cols_ref[...] + 0.5 * dot(hidden_ref[...], buf[...].reshape(-1, buf.shape[2]), 1, 1)
-
-
-def own_part(at, hidden, w, cols, n):
-    spread, _, deep, units = w.shape
+    )(place, x, gate, up, down)
+
+
+def own_body(n, place_ref, hidden_ref, down_ref, cols_ref, out_ref):
+    out_ref[...] = cols_ref[...] + 0.5 * product(hidden_ref[...], down_ref, place_ref[0], n)
+
+
+def own_part(place, hidden, down, cols, n):
     rows, share = cols.shape
-    vmem = pl.BlockSpec(memory_space=pltpu.VMEM)
-    return pl.pallas_call(
-        own_body,
+    units = hidden.shape[1]
+    vmem = pl.BlockSpec(memory_space=pltpu.VMEM)
+    return pl.pallas_call(
+        functools.partial(own_body, n),
         out_shape=jax.ShapeDtypeStruct((rows, share), f32),
-        in_specs=[pl.BlockSpec(memory_space=pltpu.SMEM), pl.BlockSpec(memory_space=pltpu.HBM), vmem, vmem],
+        in_specs=[pl.BlockSpec(memory_space=pltpu.SMEM)] + [vmem] * 3,
         out_specs=vmem,
-        scratch_shapes=[pltpu.VMEM((spread // n, deep, units), bf16), pltpu.SemaphoreType.DMA],
-        compiler_params=pltpu.CompilerParams(vmem_limit_bytes=8 * MIB),
+        compiler_params=pltpu.CompilerParams(vmem_limit_bytes=14 * MIB),
         cost_estimate=pl.CostEstimate(flops=2 * rows * share * units, transcendentals=0, bytes_accessed=2 * share * units),
         name="own",
-    )(at, w, hidden, cols)
-
-
-def sides_body(n, at_ref, w_ref, hidden_ref, low_ref, high_ref, up_ref, down_ref, buf, sem):
-    part = buf.shape[1]
+    )(place, hidden, down, cols)
+
+
+def sides_body(n, place_ref, hidden_ref, down_ref, low_ref, high_ref, next_ref, prev_ref):
     half = low_ref.shape[0]
-    copies = []
-    for i, k in enumerate((1, n - 1)):
-        j = (at_ref[0] + k) % n
-        copies.append(pltpu.make_async_copy(w_ref.at[pl.ds(j * part, part), 2], buf.at[i], sem.at[i]))
-        copies[i].start()
-    copies[0].wait()
-    piece = dot(hidden_ref[...], buf[0].reshape(-1, buf.shape[3]), 1, 1)
-    up_ref[:half] = (piece[:half] + low_ref[...].astype(f32)).astype(bf16)
-    up_ref[half:] = piece[half:].astype(bf16)
-    copies[1].wait()
-    piece = dot(hidden_ref[...], buf[1].reshape(-1, buf.shape[3]), 1, 1)
-    down_ref[:half] = piece[:half].astype(bf16)
-    down_ref[half:] = (piece[half:] + high_ref[...].astype(f32)).astype(bf16)
-
-
-def side_parts(at, hidden, w, low, high, n):
-    spread, _, deep, units = w.shape
-    rows = hidden.shape[0]
+    piece = product(hidden_ref[...], down_ref, (place_ref[0] + 1) % n, n)
+    next_ref[:half] = (piece[:half] + low_ref[...].astype(f32)).astype(bf16)
+    next_ref[half:] = piece[half:].astype(bf16)
+    piece = product(hidden_ref[...], down_ref, (place_ref[0] + n - 1) % n, n)
+    prev_ref[:half] = piece[:half].astype(bf16)
+    prev_ref[half:] = (piece[half:] + high_ref[...].astype(f32)).astype(bf16)
+
+
+def side_parts(place, hidden, down, low, high, n):
+    rows, units = hidden.shape
     share = low.shape[1]
     vmem = pl.BlockSpec(memory_space=pltpu.VMEM)
     piece = jax.ShapeDtypeStruct((rows, share), bf16)
     return pl.pallas_call(
         functools.partial(sides_body, n),
         out_shape=(piece, piece),
-        in_specs=[pl.BlockSpec(memory_space=pltpu.SMEM), pl.BlockSpec(memory_space=pltpu.HBM), vmem, vmem, vmem],
+        in_specs=[pl.BlockSpec(memory_space=pltpu.SMEM)] + [vmem] * 4,
         out_specs=(vmem, vmem),
-        scratch_shapes=[pltpu.VMEM((2, spread // n, deep, units), bf16), pltpu.SemaphoreType.DMA((2,))],
-        compiler_params=pltpu.CompilerParams(vmem_limit_bytes=12 * MIB),
+        compiler_params=pltpu.CompilerParams(vmem_limit_bytes=16 * MIB),
         cost_estimate=pl.CostEstimate(flops=4 * rows * share * units, transcendentals=0, bytes_accessed=4 * share * units),
         name="sides",
-    )(at, w, hidden, low, high)
+    )(place, hidden, down, low, high)
 
 
 def local(
@@ -469,21 +479,23 @@
     consts = (wa**-0.5 * log2e, wb**-0.5 * log2e)
     n = lax.axis_size("tp")
     share = residual.shape[1] // n
-    at = lax.axis_index("tp").astype(jnp.int32)[None]
-    at, keys_a = lax.optimization_barrier((at, keys_a))
+    where = jnp.stack([lax.axis_index("tp"), lax.axis_index("sp")]).astype(jnp.int32)
+    where, keys_a = lax.optimization_barrier((where, keys_a))
+    deep, units = w_gate.shape
 
     kv, q = pack(((keys_a, keys_b, values_a, values_b), 1), ((queries_a, queries_b), 1))
     near = [kv, along_z(kv, 1), None, along_z(kv, 3)]
-    queries = [q] + [along_y(q, k) for k in range(1, 4)]
+    queries = [q] + [along_y(q, k) for k in (1, 2, 3)]
+    first, second = pack(((w_gate, w_down.T), 0), ((w_up,), 0))
+    firsts = [first] + [along_y(first, k) for k in (1, 2, 3)]
+    seconds = [second] + [along_z(second, k) for k in (1, 2, 3)]
     kv_far = other_core(kv)
+    near[2] = along_z(kv, 2)
     (oo,) = pack(((out_a, out_b), 0))
-    outs = [oo] + [along_x(oo, k) for k in range(1, 4)]
-    (three,) = pack(((w_gate, w_up, w_down.T), 0))
-    three, queries[1], queries[3] = lax.optimization_barrier((three, queries[1], queries[3]))
-    weights = lax.all_gather(three, "sp", axis=0, tiled=True)
-    weights = in_hbm(weights.reshape(-1, 3, *w_gate.shape))
-    kv, queries[1] = lax.optimization_barrier((kv, queries[1]))
-    near[2] = along_z(kv, 2)
+    outs = [oo] + [along_x(oo, k) for k in (1, 2, 3)]
+    first, second = pack((firsts, 0), (seconds, 0), fixed=False)
+    firsts = [first] + [along_z(first, k) for k in (1, 2, 3)]
+    seconds = [second] + [along_y(second, k) for k in (1, 2, 3)]
 
     go = functools.partial(attend, consts=consts, wa=wa, wb=wb, vd=vd)
     pairs = [[queries[k] for k in g] for g in ((2, 1), (3, 0))]
@@ -497,16 +509,25 @@
     back[2], back[1] = go([[queries[2], queries[1]]], last, state, (0, 0, True))
     (back[3],) = go([[queries[3]]], last, state, (1, 0, True))
     back = {k: along_y(back[k], -k) for k in (2, 1, 3)}
-    own = go([[queries[0]]], last, state, (1, 1, False))
+    own = list(go([[queries[0]]], last, state, (1, 1, False)))
+    late = firsts[2]
+    *mid, own[1] = lax.optimization_barrier((firsts[0], firsts[1], firsts[3], *seconds, own[1]))
+    seconds = mid[3:] + [other_core(a) for a in mid[3:]]
+    others = [other_core(a) for a in mid[:3]]
     heads = merge(own, [back[k] for k in (1, 3, 2)], mix_lambda, head_gain, consts, vd)
 
-    everyone = [heads] + [along_x(heads, k) for k in range(1, 4)]
-    normed, cols = project(at, everyone, outs, residual, norm_gain[None], share)
-    hidden, low, high = hidden_of(at, normed, weights, n)
+    heads, late = lax.optimization_barrier((heads, late))
+    everyone = [heads] + [along_x(heads, k) for k in (1, 2, 3)]
+    firsts = [mid[0], mid[1], late, mid[2], others[0], others[1], other_core(late), others[2]]
+    firsts = [a.reshape(4, 2 * deep, units) for a in firsts]
+    seconds = [a.reshape(4, deep, units) for a in seconds]
+    gate, up, down = assemble(where, firsts, seconds, n)
+    normed, cols = project(where, everyone, outs, residual, norm_gain[None], share)
+    hidden, low, high = hidden_of(where, normed, gate, up, down, n)
     low, high = along_x(low, 1), along_x(high, -1)
-    mine = own_part(at, hidden, weights, cols, n)
-    up, down = side_parts(at, hidden, weights, low, high, n)
-    arrived = along_x(up, 1).astype(f32) + along_x(down, -1).astype(f32)
+    mine = own_part(where, hidden, down, cols, n)
+    ahead, behind = side_parts(where, hidden, down, low, high, n)
+    arrived = along_x(ahead, 1).astype(f32) + along_x(behind, -1).astype(f32)
     return (mine + 0.5 * arrived).astype(bf16)
 
 

time: 172 us -> 241 us (1.40)
  the two profiles are of different devices: /device:TPU:14 before, /device:TPU:0 now
where the time goes in v1:
time: 241 us; the launch traced here: 240 us
  Pallas kernels  78.6 us (33%)
  waiting for transfers between devices  78.5 us (33%)
  starting transfers between devices  76.4 us (32%)
  local copies, waits for them, and re-layouts  5 us (2%)
    ppermute x10, waiting for transfers between devices, along_x(): return lax.ppermute(x, 'tp', [(i, (i + k) % 4) for i in range(4)])  44.5 us
    pallas_call x5, Pallas kernels, attend(): pl.pallas_call(functools.partial(attend_body, groups, m, nk, state is not...  36 us
    ppermute x9, starting transfers between devices, along_z(): lax.ppermute(x, 'sp', [(place(z, y, c), place(z + k, y, c)) for z, y, c i...  35.9 us
    ppermute x12, waiting for transfers between devices, along_y(): lax.ppermute(x, 'sp', [(place(z, y, c), place(z, y + k, c)) for z, y, c i...  27.4 us
    pallas_call x1, Pallas kernels, assemble(): pl.pallas_call(functools.partial(assemble_body, n), out_shape=(shape,) *...  23.5 us
    ppermute x12, starting transfers between devices, along_y(): lax.ppermute(x, 'sp', [(place(z, y, c), place(z, y + k, c)) for z, y, c i...  20.6 us
    ppermute x10, starting transfers between devices, along_x(): return lax.ppermute(x, 'tp', [(i, (i + k) % 4) for i in range(4)])  17.6 us
    pallas_call x1, Pallas kernels, hidden_of(): pl.pallas_call(functools.partial(hidden_body, n), out_shape=(jax.ShapeDty...  7.16 us
  transfers between devices with their start and end apart: 43, of which 17 were waited for; matrix products, arithmetic and copies ran while one was open for 0% of the time, Pallas kernels for 19%

profile of v1, /device:TPU:0, one launch (start us, length us, event | category | flops | bytes accessed | tf_op | source)
XLA Modules:
  0.0 239.8 jit_solution(563438826391415366)
XLA Ops:
  1.3 3.4 %collective-permute-start.2 = (bf16[384,384]{1,0:T(8,128)(2,1)S(1)}, bf16[384,384]{1,0:T(8,128)(2,1)S(1)}, u32[]{:S(2)}, u32[]{:S(2)}) collective-permute-start(bf16[384,384]{1,0:T(8,128)(2,1)S(1)} %get-tuple-element.50.refs_3_.refs_0_), channel_id=1, source_target_pairs={{0,16},{4,20},{8,24},{12,28},{16,0},{20,4},{24,8},{28,12},{32,48},... | collective-permute-start | bytes 884744 | tf_op jit(solution)/shard_map/ppermute | solution.py:24
  5.4 2.6 %collective-permute-start.4 = (bf16[384,384]{1,0:T(8,128)(2,1)S(1)}, bf16[384,384]{1,0:T(8,128)(2,1)S(1)}, u32[]{:S(2)}, u32[]{:S(2)}) collective-permute-start(bf16[384,384]{1,0:T(8,128)(2,1)S(1)} %get-tuple-element.50.refs_3_.refs_0_), channel_id=1, source_target_pairs={{0,24},{4,28},{8,0},{12,4},{16,8},{20,12},{24,16},{28,20},{32,56},... | collective-permute-start | bytes 884744 | tf_op jit(solution)/shard_map/ppermute | solution.py:24
  9.9 3.0 %collective-permute-done.2.refs_0_ = bf16[384,384]{1,0:T(8,128)(2,1)S(1)} collective-permute-done((bf16[384,384]{1,0:T(8,128)(2,1)S(1)}, bf16[384,384]{1,0:T(8,128)(2,1)S(1)}, u32[]{:S(2)}, u32[]{:S(2)}) %collective-permute-start.2) | collective-permute-done | bytes 294944 | tf_op jit(solution)/shard_map/ppermute | solution.py:24
  12.9 4.1 %collective-permute-start.1 = (bf16[384,640]{1,0:T(8,128)(2,1)S(1)}, bf16[384,640]{1,0:T(8,128)(2,1)S(1)}, u32[]{:S(2)}, u32[]{:S(2)}) collective-permute-start(bf16[384,640]{1,0:T(8,128)(2,1)S(1)} %get-tuple-element.51.refs_4_), channel_id=1, source_target_pairs={{0,96},{4,100},{8,104},{12,108},{16,112},{20,116},{24,120},{28,124... | collective-permute-start | bytes 1474568 | tf_op jit(solution)/shard_map/ppermute | solution.py:28
  18.1 3.9 %collective-permute-start.8 = (bf16[384,640]{1,0:T(8,128)(2,1)S(1)}, bf16[384,640]{1,0:T(8,128)(2,1)S(1)}, u32[]{:S(2)}, u32[]{:S(2)}) collective-permute-start(bf16[384,640]{1,0:T(8,128)(2,1)S(1)} %get-tuple-element.51.refs_4_), channel_id=1, source_target_pairs={{0,64},{4,68},{8,72},{12,76},{16,80},{20,84},{24,88},{28,92},{32,9... | collective-permute-start | bytes 1474568 | tf_op jit(solution)/shard_map/ppermute | solution.py:28
  26.0 8.1 %attend.5 = (f32[2,512,768]{2,1,0:T(8,128)S(1)}, f32[2,16,768]{2,1,0:T(8,128)S(1)}) custom-call(bf16[384,384]{1,0:T(8,128)(2,1)S(1)} %collective-permute-done.2.refs_0_, bf16[384,384]{1,0:T(8,128)(2,1)S(1)} %collective-permute-done.3.refs_1_, bf16[384,384]{1,0:T(8,128)(2,1)S(1)} %collective-permute-done.4.refs_2_.refs_0_, ...), custom_call_target="tpu_custom_call" | custom-call | flops 2415919104 | bytes 983040 | tf_op jit(solution)/shard_map/attend/pallas_call | solution.py:250
  36.0 3.0 %collective-permute-start.12 = (bf16[128,1408]{1,0:T(8,128)(2,1)S(1)}, bf16[128,1408]{1,0:T(8,128)(2,1)S(1)}, u32[]{:S(2)}, u32[]{:S(2)}) collective-permute-start(bf16[128,1408]{1,0:T(8,128)(2,1)S(1)} %get-tuple-element.64.refs_0_), channel_id=1, source_target_pairs={{0,24},{4,28},{8,0},{12,4},{16,8},{20,12},{24,16},{28,20},{32,56},... | collective-permute-start | bytes 1081352 | tf_op jit(solution)/shard_map/ppermute | solution.py:24
  40.5 2.3 collective-permute-start.15
  42.8 8.2 %attend.6 = (f32[2,512,768]{2,1,0:T(8,128)S(1)}, f32[2,16,768]{2,1,0:T(8,128)S(1)}) custom-call(bf16[384,384]{1,0:T(8,128)(2,1)S(1)} %collective-permute-done.2.refs_0_, bf16[384,384]{1,0:T(8,128)(2,1)S(1)} %collective-permute-done.3.refs_1_, bf16[384,384]{1,0:T(8,128)(2,1)S(1)} %collective-permute-done.4.refs_2_.refs_0_, ...), custom_call_target="tpu_custom_call" | custom-call | flops 2415919104 | bytes 983040 | tf_op jit(solution)/shard_map/attend/pallas_call | solution.py:250
  54.6 3.1 %collective-permute-start.19 = (bf16[256,1408]{1,0:T(8,128)(2,1)S(1)}, bf16[256,1408]{1,0:T(8,128)(2,1)S(1)}, u32[]{:S(2)}, u32[]{:S(2)}) collective-permute-start(bf16[256,1408]{1,0:T(8,128)(2,1)S(1)} %get-tuple-element.78), channel_id=1, source_target_pairs={{0,16},{4,20},{8,24},{12,28},{16,0},{20,4},{24,8},{28,12},{32,48},... | collective-permute-start | bytes 2162696 | tf_op jit(solution)/shard_map/ppermute | solution.py:24
  57.8 2.9 %collective-permute-start.17 = (bf16[512,1408]{1,0:T(8,128)(2,1)S(1)}, bf16[512,1408]{1,0:T(8,128)(2,1)S(1)}, u32[]{:S(2)}, u32[]{:S(2)}) collective-permute-start(bf16[512,1408]{1,0:T(8,128)(2,1)S(1)} %get-tuple-element.74), channel_id=1, source_target_pairs={{0,96},{4,100},{8,104},{12,108},{16,112},{20,116},{24,120},{28,124... | collective-permute-start | bytes 4325384 | tf_op jit(solution)/shard_map/ppermute | solution.py:28
  60.9 12.2 %collective-permute-done.18 = bf16[256,1408]{1,0:T(8,128)(2,1)S(1)} collective-permute-done((bf16[256,1408]{1,0:T(8,128)(2,1)S(1)}, bf16[256,1408]{1,0:T(8,128)(2,1)S(1)}, u32[]{:S(2)}, u32[]{:S(2)}) %collective-permute-start.18) | collective-permute-done | bytes 720928 | tf_op jit(solution)/shard_map/ppermute | solution.py:24
  73.1 18.1 %collective-permute-start.24 = (bf16[512,1408]{1,0:T(8,128)(2,1)S(1)}, bf16[512,1408]{1,0:T(8,128)(2,1)S(1)}, u32[]{:S(2)}, u32[]{:S(2)}) collective-permute-start(bf16[512,1408]{1,0:T(8,128)(2,1)S(1)} %get-tuple-element.74), channel_id=1, source_target_pairs={{0,64},{4,68},{8,72},{12,76},{16,80},{20,84},{24,88},{28,92},{32,9... | collective-permute-start | bytes 4325384 | tf_op jit(solution)/shard_map/ppermute | solution.py:28
  91.1 5.4 %attend.9 = bf16[544,384]{1,0:T(8,128)(2,1)S(1)} custom-call(bf16[384,384]{1,0:T(8,128)(2,1)S(1)} %collective-permute-done.4.refs_2_.refs_0_, bf16[384,640]{1,0:T(8,128)(2,1)S(1)} %collective-permute-done.6.refs_1_.refs_2_, bf16[384,640]{1,0:T(8,128)(2,1)S(1)} %collective-permute-done.7.refs_2_.refs_3_, ...), custom_call_target="tpu_custom_call" | custom-call | flops 1207959552 | bytes 1966080 | tf_op jit(solution)/shard_map/attend/pallas_call | solution.py:250
  96.7 8.9 %attend.8 = (bf16[544,384]{1,0:T(8,128)(2,1)S(1)}, bf16[544,384]{1,0:T(8,128)(2,1)S(1)}) custom-call(bf16[384,384]{1,0:T(8,128)(2,1)S(1)} %collective-permute-done.2.refs_0_, bf16[384,384]{1,0:T(8,128)(2,1)S(1)} %collective-permute-done.3.refs_1_, bf16[384,640]{1,0:T(8,128)(2,1)S(1)} %collective-permute-done.6.refs_1_.refs_2_, ...), custom_call_target="tpu_custom_call" | custom-call | flops 2415919104 | bytes 1966080 | tf_op jit(solution)/shard_map/attend/pallas_call | solution.py:250
  105.6 3.3 %collective-permute-start.21 = (bf16[544,384]{1,0:T(8,128)(2,1)S(1)}, bf16[544,384]{1,0:T(8,128)(2,1)S(1)}, u32[]{:S(2)}, u32[]{:S(2)}) collective-permute-start(bf16[544,384]{1,0:T(8,128)(2,1)S(1)} %get-tuple-element.70), channel_id=1, source_target_pairs={{0,24},{4,28},{8,0},{12,4},{16,8},{20,12},{24,16},{28,20},{32,56},... | collective-permute-start | bytes 1253384 | tf_op jit(solution)/shard_map/ppermute | solution.py:24
  111.7 5.1 %collective-permute-done.21.refs_0_ = bf16[544,384]{1,0:T(8,128)(2,1)S(1)} collective-permute-done((bf16[544,384]{1,0:T(8,128)(2,1)S(1)}, bf16[544,384]{1,0:T(8,128)(2,1)S(1)}, u32[]{:S(2)}, u32[]{:S(2)}) %collective-permute-start.21) | collective-permute-done | bytes 417824 | tf_op jit(solution)/shard_map/ppermute | solution.py:24
  116.8 3.0 %collective-permute-start.29 = (bf16[256,2048]{1,0:T(8,128)(2,1)S(1)}, bf16[256,2048]{1,0:T(8,128)(2,1)S(1)}, u32[]{:S(2)}, u32[]{:S(2)}) collective-permute-start(bf16[256,2048]{1,0:T(8,128)(2,1)S(1)} %pack.7.refs_5_), channel_id=1, source_target_pairs={{0,2},{1,3},{2,0},{3,1},{4,6},{5,7},{6,4},{7,5},{8,10},{9,11},{10,... | collective-permute-start | bytes 3145736 | tf_op jit(solution)/shard_map/ppermute | solution.py:36
  123.2 5.4 %attend.7 = (f32[1,512,384]{2,1,0:T(8,128)S(1)}, f32[1,16,384]{2,1,0:T(8,128)S(1)}) custom-call(bf16[384,384]{1,0:T(8,128)(2,1)S(1)} %get-tuple-element.50.refs_3_.refs_0_, bf16[384,640]{1,0:T(8,128)(2,1)S(1)} %collective-permute-done.6.refs_1_.refs_2_, bf16[384,640]{1,0:T(8,128)(2,1)S(1)} %collective-permute-done.7.refs_2_.refs_3_, ...), custom_call_target="tpu_custom_call" | custom-call | flops 1207959552 | bytes 1966080 | tf_op jit(solution)/shard_map/attend/pallas_call | solution.py:250
  128.6 5.9 %collective-permute-done.23.refs_2_ = bf16[544,384]{1,0:T(8,128)(2,1)S(1)} collective-permute-done((bf16[544,384]{1,0:T(8,128)(2,1)S(1)}, bf16[544,384]{1,0:T(8,128)(2,1)S(1)}, u32[]{:S(2)}, u32[]{:S(2)}) %collective-permute-start.23) | collective-permute-done | bytes 417824 | tf_op jit(solution)/shard_map/ppermute | solution.py:24
  137.7 23.2 %collective-permute-done.29.refs_7_ = bf16[256,2048]{1,0:T(8,128)(2,1)S(1)} collective-permute-done((bf16[256,2048]{1,0:T(8,128)(2,1)S(1)}, bf16[256,2048]{1,0:T(8,128)(2,1)S(1)}, u32[]{:S(2)}, u32[]{:S(2)}) %collective-permute-start.29) | collective-permute-done | bytes 1048608 | tf_op jit(solution)/shard_map/ppermute | solution.py:36
  161.8 4.3 %collective-permute-done.30.refs_8_ = bf16[256,2048]{1,0:T(8,128)(2,1)S(1)} collective-permute-done((bf16[256,2048]{1,0:T(8,128)(2,1)S(1)}, bf16[256,2048]{1,0:T(8,128)(2,1)S(1)}, u32[]{:S(2)}, u32[]{:S(2)}) %collective-permute-start.30) | collective-permute-done | bytes 1048608 | tf_op jit(solution)/shard_map/ppermute | solution.py:36
  166.1 2.6 %collective-permute-start.27 = (bf16[384,256]{1,0:T(8,128)(2,1)S(1)}, bf16[384,256]{1,0:T(8,128)(2,1)S(1)}, u32[]{:S(2)}, u32[]{:S(2)}) collective-permute-start(bf16[384,256]{1,0:T(8,128)(2,1)S(1)} %merge.1.refs_1_), channel_id=1, source_target_pairs={{0,3},{1,0},{2,1},{3,2},{4,7},{5,4},{6,5},{7,6},{8,11},{9,8},{10,9... | collective-permute-start | bytes 589832 | tf_op jit(solution)/shard_map/ppermute | solution.py:36
  169.2 3.8 %collective-permute-done.27.refs_4_ = bf16[384,256]{1,0:T(8,128)(2,1)S(1)} collective-permute-done((bf16[384,256]{1,0:T(8,128)(2,1)S(1)}, bf16[384,256]{1,0:T(8,128)(2,1)S(1)}, u32[]{:S(2)}, u32[]{:S(2)}) %collective-permute-start.27) | collective-permute-done | bytes 196640 | tf_op jit(solution)/shard_map/ppermute | solution.py:36
  175.4 2.9 %project.1 = (bf16[384,2048]{1,0:T(8,128)(2,1)S(1)}, f32[384,512]{1,0:T(8,128)S(1)}) custom-call(s32[2]{0:T(128)S(1)} %pad_add_fusion.refs_0_.place_ref, bf16[384,256]{1,0:T(8,128)(2,1)S(1)} %merge.1.refs_1_, bf16[384,256]{1,0:T(8,128)(2,1)S(1)} %collective-permute-done.25.refs_2_, bf16[384,256]{1,0:T(8,128)(2,1)S(1)} %collective-permute-done.26.refs_3_, ...), custom_call_target="tpu_custom_call" | custom-call | flops 1610612736 | bytes 8388608 | tf_op jit(solution)/shard_map/project/pallas_call | solution.py:316
  178.3 2.1 collective-permute-done.38
  185.4 23.5 %assemble.1 = (bf16[32,64,1408]{2,1,0:T(8,128)(2,1)S(1)}, bf16[32,64,1408]{2,1,0:T(8,128)(2,1)S(1)}, bf16[32,64,1408]{2,1,0:T(8,128)(2,1)S(1)}) custom-call(s32[2]{0:T(128)S(1)} %pad_add_fusion.refs_0_.place_ref, bf16[4,128,1408]{2,1,0:T(8,128)(2,1)S(1)} %bitcast.21, bf16[4,128,1408]{2,1,0:T(8,128)(2,1)S(1)} %bitcast.22, bf16[4,128,1408]{2,1,0:T(8,128)(2,1)S(1)} %bitcast.24, ...), custom_call_target="tpu_custom_call" | custom-call | tf_op jit(solution)/shard_map/assemble/pallas_call | solution.py:356
  208.9 7.2 %hidden.1 = (bf16[384,1408]{1,0:T(8,128)(2,1)S(1)}, bf16[192,512]{1,0:T(8,128)(2,1)S(1)}, bf16[192,512]{1,0:T(8,128)(2,1)S(1)}) custom-call(s32[2]{0:T(128)S(1)} %pad_add_fusion.refs_0_.place_ref, bf16[384,2048]{1,0:T(8,128)(2,1)S(1)} %get-tuple-element.73.x_ref, bf16[32,64,1408]{2,1,0:T(8,128)(2,1)S(1)} %get-tuple-element.82.gate_ref, ...), custom_call_target="tpu_custom_call" | custom-call | flops 4429185024 | bytes 11534336 | tf_op jit(solution)/shard_map/hidden/pallas_call | solution.py:403
  217.4 2.5 %collective-permute-start.40 = (bf16[192,512]{1,0:T(8,128)(2,1)S(1)}, bf16[192,512]{1,0:T(8,128)(2,1)S(1)}, u32[]{:S(2)}, u32[]{:S(2)}) collective-permute-start(bf16[192,512]{1,0:T(8,128)(2,1)S(1)} %get-tuple-element.88), channel_id=1, source_target_pairs={{0,3},{1,0},{2,1},{3,2},{4,7},{5,4},{6,5},{7,6},{8,11},{9,8},{10,9... | collective-permute-start | bytes 589832 | tf_op jit(solution)/shard_map/ppermute | solution.py:36
  219.9 5.1 %collective-permute-done.39.low_ref = bf16[192,512]{1,0:T(8,128)(2,1)S(1)} collective-permute-done((bf16[192,512]{1,0:T(8,128)(2,1)S(1)}, bf16[192,512]{1,0:T(8,128)(2,1)S(1)}, u32[]{:S(2)}, u32[]{:S(2)}) %collective-permute-start.39) | collective-permute-done | bytes 196640 | tf_op jit(solution)/shard_map/ppermute | solution.py:36
  228.2 2.1 collective-permute-start.42
  231.7 7.2 %collective-permute-done.41 = bf16[384,512]{1,0:T(8,128)(2,1)S(1)} collective-permute-done((bf16[384,512]{1,0:T(8,128)(2,1)S(1)}, bf16[384,512]{1,0:T(8,128)(2,1)S(1)}, u32[]{:S(2)}, u32[]{:S(2)}) %collective-permute-start.41) | collective-permute-done | bytes 393248 | tf_op jit(solution)/shard_map/ppermute | solution.py:36
  (87 shorter events, 41.0 us)
Async XLA Ops:
  1.3 11.5 %collective-permute-start.2 = (bf16[384,384]{1,0:T(8,128)(2,1)S(1)}, bf16[384,384]{1,0:T(8,128)(2,1)S(1)}, u32[]{:S(2)}, u32[]{:S(2)}) collective-permute-start(bf16[384,384]{1,0:T(8,128)(2,1)S(1)} %get-tuple-element.50.refs_3_.refs_0_), channel_id=1, source_target_pairs={{0,16},{4,20},{8,24},{12,28},{16,0},{20,4},{24,8},{28,12},{32,48},... | collective-permute-start | bytes 884744 | tf_op jit(solution)/shard_map/ppermute | solution.py:24
  4.7 13.3 %collective-permute-start.3 = (bf16[384,384]{1,0:T(8,128)(2,1)S(1)}, bf16[384,384]{1,0:T(8,128)(2,1)S(1)}, u32[]{:S(2)}, u32[]{:S(2)}) collective-permute-start(bf16[384,384]{1,0:T(8,128)(2,1)S(1)} %get-tuple-element.50.refs_3_.refs_0_), channel_id=1, source_target_pairs={{0,8},{4,12},{8,16},{12,20},{16,24},{20,28},{24,0},{28,4},{32,40},... | collective-permute-start | bytes 884744 | tf_op jit(solution)/shard_map/ppermute | solution.py:24
  5.4 19.5 %collective-permute-start.5 = (bf16[384,640]{1,0:T(8,128)(2,1)S(1)}, bf16[384,640]{1,0:T(8,128)(2,1)S(1)}, u32[]{:S(2)}, u32[]{:S(2)}) collective-permute-start(bf16[384,640]{1,0:T(8,128)(2,1)S(1)} %get-tuple-element.51.refs_4_), channel_id=1, source_target_pairs={{0,4},{4,0},{8,12},{12,8},{16,20},{20,16},{24,28},{28,24},{32,36},... | collective-permute-start | bytes 1474568 | tf_op jit(solution)/shard_map/ppermute | solution.py:32
  5.4 17.7 %collective-permute-start.4 = (bf16[384,384]{1,0:T(8,128)(2,1)S(1)}, bf16[384,384]{1,0:T(8,128)(2,1)S(1)}, u32[]{:S(2)}, u32[]{:S(2)}) collective-permute-start(bf16[384,384]{1,0:T(8,128)(2,1)S(1)} %get-tuple-element.50.refs_3_.refs_0_), channel_id=1, source_target_pairs={{0,24},{4,28},{8,0},{12,4},{16,8},{20,12},{24,16},{28,20},{32,56},... | collective-permute-start | bytes 884744 | tf_op jit(solution)/shard_map/ppermute | solution.py:24
  8.0 26.1 %collective-permute-start = (bf16[384,640]{1,0:T(8,128)(2,1)S(1)}, bf16[384,640]{1,0:T(8,128)(2,1)S(1)}, u32[]{:S(2)}, u32[]{:S(2)}) collective-permute-start(bf16[384,640]{1,0:T(8,128)(2,1)S(1)} %get-tuple-element.51.refs_4_), channel_id=1, source_target_pairs={{0,32},{4,36},{8,40},{12,44},{16,48},{20,52},{24,56},{28,60},{32,6... | collective-permute-start | bytes 1474568 | tf_op jit(solution)/shard_map/ppermute | solution.py:28
  12.9 23.2 %collective-permute-start.1 = (bf16[384,640]{1,0:T(8,128)(2,1)S(1)}, bf16[384,640]{1,0:T(8,128)(2,1)S(1)}, u32[]{:S(2)}, u32[]{:S(2)}) collective-permute-start(bf16[384,640]{1,0:T(8,128)(2,1)S(1)} %get-tuple-element.51.refs_4_), channel_id=1, source_target_pairs={{0,96},{4,100},{8,104},{12,108},{16,112},{20,116},{24,120},{28,124... | collective-permute-start | bytes 1474568 | tf_op jit(solution)/shard_map/ppermute | solution.py:28
  18.1 22.4 %collective-permute-start.8 = (bf16[384,640]{1,0:T(8,128)(2,1)S(1)}, bf16[384,640]{1,0:T(8,128)(2,1)S(1)}, u32[]{:S(2)}, u32[]{:S(2)}) collective-permute-start(bf16[384,640]{1,0:T(8,128)(2,1)S(1)} %get-tuple-element.51.refs_4_), channel_id=1, source_target_pairs={{0,64},{4,68},{8,72},{12,76},{16,80},{20,84},{24,88},{28,92},{32,9... | collective-permute-start | bytes 1474568 | tf_op jit(solution)/shard_map/ppermute | solution.py:28
  23.1 28.5 %collective-permute-start.10 = (bf16[128,1408]{1,0:T(8,128)(2,1)S(1)}, bf16[128,1408]{1,0:T(8,128)(2,1)S(1)}, u32[]{:S(2)}, u32[]{:S(2)}) collective-permute-start(bf16[128,1408]{1,0:T(8,128)(2,1)S(1)} %get-tuple-element.64.refs_0_), channel_id=1, source_target_pairs={{0,8},{4,12},{8,16},{12,20},{16,24},{20,28},{24,0},{28,4},{32,40},... | collective-permute-start | bytes 1081352 | tf_op jit(solution)/shard_map/ppermute | solution.py:24
  24.9 14.3 %collective-permute-start.13 = (bf16[64,1408]{1,0:T(8,128)(2,1)S(1)}, bf16[64,1408]{1,0:T(8,128)(2,1)S(1)}, u32[]{:S(2)}, u32[]{:S(2)}) collective-permute-start(bf16[64,1408]{1,0:T(8,128)(2,1)S(1)} %get-tuple-element.65.refs_4_), channel_id=1, source_target_pairs={{0,32},{4,36},{8,40},{12,44},{16,48},{20,52},{24,56},{28,60},{32,6... | collective-permute-start | bytes 540680 | tf_op jit(solution)/shard_map/ppermute | solution.py:28
  34.0 17.6 %collective-permute-start.11 = (bf16[128,1408]{1,0:T(8,128)(2,1)S(1)}, bf16[128,1408]{1,0:T(8,128)(2,1)S(1)}, u32[]{:S(2)}, u32[]{:S(2)}) collective-permute-start(bf16[128,1408]{1,0:T(8,128)(2,1)S(1)} %get-tuple-element.64.refs_0_), channel_id=1, source_target_pairs={{0,16},{4,20},{8,24},{12,28},{16,0},{20,4},{24,8},{28,12},{32,48},... | collective-permute-start | bytes 1081352 | tf_op jit(solution)/shard_map/ppermute | solution.py:24
  36.0 15.7 %collective-permute-start.12 = (bf16[128,1408]{1,0:T(8,128)(2,1)S(1)}, bf16[128,1408]{1,0:T(8,128)(2,1)S(1)}, u32[]{:S(2)}, u32[]{:S(2)}) collective-permute-start(bf16[128,1408]{1,0:T(8,128)(2,1)S(1)} %get-tuple-element.64.refs_0_), channel_id=1, source_target_pairs={{0,24},{4,28},{8,0},{12,4},{16,8},{20,12},{24,16},{28,20},{32,56},... | collective-permute-start | bytes 1081352 | tf_op jit(solution)/shard_map/ppermute | solution.py:24
  39.2 11.8 %collective-permute-start.14 = (bf16[64,1408]{1,0:T(8,128)(2,1)S(1)}, bf16[64,1408]{1,0:T(8,128)(2,1)S(1)}, u32[]{:S(2)}, u32[]{:S(2)}) collective-permute-start(bf16[64,1408]{1,0:T(8,128)(2,1)S(1)} %get-tuple-element.65.refs_4_), channel_id=1, source_target_pairs={{0,64},{4,68},{8,72},{12,76},{16,80},{20,84},{24,88},{28,92},{32,9... | collective-permute-start | bytes 540680 | tf_op jit(solution)/shard_map/ppermute | solution.py:28
  40.5 10.6 %collective-permute-start.15 = (bf16[64,1408]{1,0:T(8,128)(2,1)S(1)}, bf16[64,1408]{1,0:T(8,128)(2,1)S(1)}, u32[]{:S(2)}, u32[]{:S(2)}) collective-permute-start(bf16[64,1408]{1,0:T(8,128)(2,1)S(1)} %get-tuple-element.65.refs_4_), channel_id=1, source_target_pairs={{0,96},{4,100},{8,104},{12,108},{16,112},{20,116},{24,120},{28,124... | collective-permute-start | bytes 540680 | tf_op jit(solution)/shard_map/ppermute | solution.py:28
  53.3 19.8 %collective-permute-start.18 = (bf16[256,1408]{1,0:T(8,128)(2,1)S(1)}, bf16[256,1408]{1,0:T(8,128)(2,1)S(1)}, u32[]{:S(2)}, u32[]{:S(2)}) collective-permute-start(bf16[256,1408]{1,0:T(8,128)(2,1)S(1)} %get-tuple-element.78), channel_id=1, source_target_pairs={{0,8},{4,12},{8,16},{12,20},{16,24},{20,28},{24,0},{28,4},{32,40},... | collective-permute-start | bytes 2162696 | tf_op jit(solution)/shard_map/ppermute | solution.py:24
  54.4 65.5 %collective-permute-start.16 = (bf16[512,1408]{1,0:T(8,128)(2,1)S(1)}, bf16[512,1408]{1,0:T(8,128)(2,1)S(1)}, u32[]{:S(2)}, u32[]{:S(2)}) collective-permute-start(bf16[512,1408]{1,0:T(8,128)(2,1)S(1)} %get-tuple-element.74), channel_id=1, source_target_pairs={{0,32},{4,36},{8,40},{12,44},{16,48},{20,52},{24,56},{28,60},{32,6... | collective-permute-start | bytes 4325384 | tf_op jit(solution)/shard_map/ppermute | solution.py:28
  54.6 41.9 %collective-permute-start.19 = (bf16[256,1408]{1,0:T(8,128)(2,1)S(1)}, bf16[256,1408]{1,0:T(8,128)(2,1)S(1)}, u32[]{:S(2)}, u32[]{:S(2)}) collective-permute-start(bf16[256,1408]{1,0:T(8,128)(2,1)S(1)} %get-tuple-element.78), channel_id=1, source_target_pairs={{0,16},{4,20},{8,24},{12,28},{16,0},{20,4},{24,8},{28,12},{32,48},... | collective-permute-start | bytes 2162696 | tf_op jit(solution)/shard_map/ppermute | solution.py:24
  57.8 64.8 %collective-permute-start.17 = (bf16[512,1408]{1,0:T(8,128)(2,1)S(1)}, bf16[512,1408]{1,0:T(8,128)(2,1)S(1)}, u32[]{:S(2)}, u32[]{:S(2)}) collective-permute-start(bf16[512,1408]{1,0:T(8,128)(2,1)S(1)} %get-tuple-element.74), channel_id=1, source_target_pairs={{0,96},{4,100},{8,104},{12,108},{16,112},{20,116},{24,120},{28,124... | collective-permute-start | bytes 4325384 | tf_op jit(solution)/shard_map/ppermute | solution.py:28
  60.7 44.9 %collective-permute-start.20 = (bf16[256,1408]{1,0:T(8,128)(2,1)S(1)}, bf16[256,1408]{1,0:T(8,128)(2,1)S(1)}, u32[]{:S(2)}, u32[]{:S(2)}) collective-permute-start(bf16[256,1408]{1,0:T(8,128)(2,1)S(1)} %get-tuple-element.78), channel_id=1, source_target_pairs={{0,24},{4,28},{8,0},{12,4},{16,8},{20,12},{24,16},{28,20},{32,56},... | collective-permute-start | bytes 2162696 | tf_op jit(solution)/shard_map/ppermute | solution.py:24
  73.1 61.5 %collective-permute-start.24 = (bf16[512,1408]{1,0:T(8,128)(2,1)S(1)}, bf16[512,1408]{1,0:T(8,128)(2,1)S(1)}, u32[]{:S(2)}, u32[]{:S(2)}) collective-permute-start(bf16[512,1408]{1,0:T(8,128)(2,1)S(1)} %get-tuple-element.74), channel_id=1, source_target_pairs={{0,64},{4,68},{8,72},{12,76},{16,80},{20,84},{24,88},{28,92},{32,9... | collective-permute-start | bytes 4325384 | tf_op jit(solution)/shard_map/ppermute | solution.py:28
  96.6 13.6 %collective-permute-start.22 = (bf16[544,384]{1,0:T(8,128)(2,1)S(1)}, bf16[544,384]{1,0:T(8,128)(2,1)S(1)}, u32[]{:S(2)}, u32[]{:S(2)}) collective-permute-start(bf16[544,384]{1,0:T(8,128)(2,1)S(1)} %attend.9), channel_id=1, source_target_pairs={{0,8},{4,12},{8,16},{12,20},{16,24},{20,28},{24,0},{28,4},{32,40},... | collective-permute-start | bytes 1253384 | tf_op jit(solution)/shard_map/ppermute | solution.py:24
  105.6 11.2 %collective-permute-start.21 = (bf16[544,384]{1,0:T(8,128)(2,1)S(1)}, bf16[544,384]{1,0:T(8,128)(2,1)S(1)}, u32[]{:S(2)}, u32[]{:S(2)}) collective-permute-start(bf16[544,384]{1,0:T(8,128)(2,1)S(1)} %get-tuple-element.70), channel_id=1, source_target_pairs={{0,24},{4,28},{8,0},{12,4},{16,8},{20,12},{24,16},{28,20},{32,56},... | collective-permute-start | bytes 1253384 | tf_op jit(solution)/shard_map/ppermute | solution.py:24
  110.1 26.3 %collective-permute-start.28 = (bf16[256,2048]{1,0:T(8,128)(2,1)S(1)}, bf16[256,2048]{1,0:T(8,128)(2,1)S(1)}, u32[]{:S(2)}, u32[]{:S(2)}) collective-permute-start(bf16[256,2048]{1,0:T(8,128)(2,1)S(1)} %pack.7.refs_5_), channel_id=1, source_target_pairs={{0,1},{1,2},{2,3},{3,0},{4,5},{5,6},{6,7},{7,4},{8,9},{9,10},{10,1... | collective-permute-start | bytes 3145736 | tf_op jit(solution)/shard_map/ppermute | solution.py:36
  116.8 44.1 %collective-permute-start.29 = (bf16[256,2048]{1,0:T(8,128)(2,1)S(1)}, bf16[256,2048]{1,0:T(8,128)(2,1)S(1)}, u32[]{:S(2)}, u32[]{:S(2)}) collective-permute-start(bf16[256,2048]{1,0:T(8,128)(2,1)S(1)} %pack.7.refs_5_), channel_id=1, source_target_pairs={{0,2},{1,3},{2,0},{3,1},{4,6},{5,7},{6,4},{7,5},{8,10},{9,11},{10,... | collective-permute-start | bytes 3145736 | tf_op jit(solution)/shard_map/ppermute | solution.py:36
  119.9 46.2 %collective-permute-start.30 = (bf16[256,2048]{1,0:T(8,128)(2,1)S(1)}, bf16[256,2048]{1,0:T(8,128)(2,1)S(1)}, u32[]{:S(2)}, u32[]{:S(2)}) collective-permute-start(bf16[256,2048]{1,0:T(8,128)(2,1)S(1)} %pack.7.refs_5_), channel_id=1, source_target_pairs={{0,3},{1,0},{2,1},{3,2},{4,7},{5,4},{6,5},{7,6},{8,11},{9,8},{10,9... | collective-permute-start | bytes 3145736 | tf_op jit(solution)/shard_map/ppermute | solution.py:36
  122.6 12.0 %collective-permute-start.23 = (bf16[544,384]{1,0:T(8,128)(2,1)S(1)}, bf16[544,384]{1,0:T(8,128)(2,1)S(1)}, u32[]{:S(2)}, u32[]{:S(2)}) collective-permute-start(bf16[544,384]{1,0:T(8,128)(2,1)S(1)} %get-tuple-element.71), channel_id=1, source_target_pairs={{0,16},{4,20},{8,24},{12,28},{16,0},{20,4},{24,8},{28,12},{32,48},... | collective-permute-start | bytes 1253384 | tf_op jit(solution)/shard_map/ppermute | solution.py:24
  134.6 38.5 %collective-permute-start.35 = (bf16[256,1408]{1,0:T(8,128)(2,1)S(1)}, bf16[256,1408]{1,0:T(8,128)(2,1)S(1)}, u32[]{:S(2)}, u32[]{:S(2)}) collective-permute-start(bf16[256,1408]{1,0:T(8,128)(2,1)S(1)} %get-tuple-element.78), channel_id=1, source_target_pairs={{0,4},{4,0},{8,12},{12,8},{16,20},{20,16},{24,28},{28,24},{32,36},... | collective-permute-start | bytes 2162696 | tf_op jit(solution)/shard_map/ppermute | solution.py:32
  134.6 39.0 %collective-permute-start.36 = (bf16[256,1408]{1,0:T(8,128)(2,1)S(1)}, bf16[256,1408]{1,0:T(8,128)(2,1)S(1)}, u32[]{:S(2)}, u32[]{:S(2)}) collective-permute-start(bf16[256,1408]{1,0:T(8,128)(2,1)S(1)} %collective-permute-done.18), channel_id=1, source_target_pairs={{0,4},{4,0},{8,12},{12,8},{16,20},{20,16},{24,28},{28,24},{32,36},... | collective-permute-start | bytes 2162696 | tf_op jit(solution)/shard_map/ppermute | solution.py:32
  136.5 32.3 %collective-permute-start.25 = (bf16[384,256]{1,0:T(8,128)(2,1)S(1)}, bf16[384,256]{1,0:T(8,128)(2,1)S(1)}, u32[]{:S(2)}, u32[]{:S(2)}) collective-permute-start(bf16[384,256]{1,0:T(8,128)(2,1)S(1)} %merge.1.refs_1_), channel_id=1, source_target_pairs={{0,1},{1,2},{2,3},{3,0},{4,5},{5,6},{6,7},{7,4},{8,9},{9,10},{10,1... | collective-permute-start | bytes 589832 | tf_op jit(solution)/shard_map/ppermute | solution.py:36
  168.7 11.7 %collective-permute-start.33 = (bf16[512,1408]{1,0:T(8,128)(2,1)S(1)}, bf16[512,1408]{1,0:T(8,128)(2,1)S(1)}, u32[]{:S(2)}, u32[]{:S(2)}) collective-permute-start(bf16[512,1408]{1,0:T(8,128)(2,1)S(1)} %collective-permute-done.24), channel_id=1, source_target_pairs={{0,4},{4,0},{8,12},{12,8},{16,20},{20,16},{24,28},{28,24},{32,36},... | collective-permute-start | bytes 4325384 | tf_op jit(solution)/shard_map/ppermute | solution.py:32
  168.7 11.7 %collective-permute-start.32 = (bf16[512,1408]{1,0:T(8,128)(2,1)S(1)}, bf16[512,1408]{1,0:T(8,128)(2,1)S(1)}, u32[]{:S(2)}, u32[]{:S(2)}) collective-permute-start(bf16[512,1408]{1,0:T(8,128)(2,1)S(1)} %collective-permute-done.16), channel_id=1, source_target_pairs={{0,4},{4,0},{8,12},{12,8},{16,20},{20,16},{24,28},{28,24},{32,36},... | collective-permute-start | bytes 4325384 | tf_op jit(solution)/shard_map/ppermute | solution.py:32
  227.0 11.9 %collective-permute-start.41 = (bf16[384,512]{1,0:T(8,128)(2,1)S(1)}, bf16[384,512]{1,0:T(8,128)(2,1)S(1)}, u32[]{:S(2)}, u32[]{:S(2)}) collective-permute-start(bf16[384,512]{1,0:T(8,128)(2,1)S(1)} %get-tuple-element.89), channel_id=1, source_target_pairs={{0,1},{1,2},{2,3},{3,0},{4,5},{5,6},{6,7},{7,4},{8,9},{9,10},{10,1... | collective-permute-start | bytes 1179656 | tf_op jit(solution)/shard_map/ppermute | solution.py:36
  228.2 10.7 %collective-permute-start.42 = (bf16[384,512]{1,0:T(8,128)(2,1)S(1)}, bf16[384,512]{1,0:T(8,128)(2,1)S(1)}, u32[]{:S(2)}, u32[]{:S(2)}) collective-permute-start(bf16[384,512]{1,0:T(8,128)(2,1)S(1)} %get-tuple-element.90), channel_id=1, source_target_pairs={{0,3},{1,0},{2,1},{3,2},{4,7},{5,4},{6,5},{7,6},{8,11},{9,8},{10,9... | collective-permute-start | bytes 1179656 | tf_op jit(solution)/shard_map/ppermute | solution.py:36
  (19 other events, 196.6 us)
